TPU v7x, 512 devices: a whole 4x4x16 slice. The times are simulated.
512 devices in a mesh: ep: 32 (over z, core), tp: 16 (over y, x).
Axes of the slice: x: 4, y: 4, z: 16, core: 2. Of those that a mesh axis runs over, the one named last changes fastest.
Arguments:
- queries: bfloat16 [8192, 2048], P('ep', 'tp'), may hold values from -6 to 6
- keys: bfloat16 [8192, 2048], P('ep', 'tp'), may hold values from -6 to 6
- values: bfloat16 [8192, 2048], P('ep', 'tp'), may hold values from -6 to 6
- gates: bfloat16 [8192, 2048], P('ep', 'tp'), may hold values from -6 to 6
- log_decay: float32 [8192, 16], P('ep', 'tp'), may hold values from -2 to 0
- out_weight: bfloat16 [2048, 2048], P(None, 'tp'), may hold values from -0.125 to 0.125
- moe_rows: bfloat16 [8192, 2048], P('ep'), may hold values from -140 to 140
- moe_gain: bfloat16 [2048], replicated, may hold values from 0.099609375 to 1.8984375
- routes: int32 [8192, 2], P('ep'), may hold values from 0 to 31, as said below
- route_weights: float32 [8192, 2], P('ep'), may hold values from 0.1 to 1
- gate_proj: bfloat16 [32, 2048, 4096], P('ep', None, 'tp'), may hold values from -0.125 to 0.125
- up_proj: bfloat16 [32, 2048, 4096], P('ep', None, 'tp'), may hold values from -0.125 to 0.125
- down_proj: bfloat16 [32, 4096, 2048], P('ep', None, 'tp'), may hold values from -0.09375 to 0.09375
Outputs:
- mixer_out: bfloat16 [8192, 2048], P('ep', 'tp')
- moe_out: bfloat16 [8192, 2048], P('ep', 'tp')
Inputs may be any that keep to these rules, and one draw needn't show every extreme that they name: `routes`: each row names two different experts of one group of 8 consecutive experts; in each aligned block of 256 rows every expert is named by exactly 16 rows.
All inputs are finite; a program needn't handle non-finite values.
Results may differ from a plain program's by a relative error of at most 0.011.
Values may be sent and summed in bfloat16 or wider, within the bound.
A program may use at most 64 MiB of HBM per device.

v0:
```python
import jax
import jax.numpy as jnp
from jax import lax
from jax.sharding import Mesh
from jax.sharding import PartitionSpec as P

BLOCK = 128
EP = ("ep_0", "ep_1")
TP = ("tp_0", "tp_1")


def filled_with(array, identity):
    return jax.tree.map(
        lambda part, zero: jnp.zeros_like(part) + jnp.asarray(zero, part.dtype), array, identity
    )


def collected_together(array, axis):
    leaves = jax.tree.leaves(array)
    turns = sorted(range(len(leaves)), key=lambda k: -leaves[k].size)
    width = (1, *leaves[turns[0]].shape)[-1]
    lines = [
        jnp.pad(leaves[k].reshape(-1), (0, -leaves[k].size % width)).reshape(-1, width)
        for k in turns
    ]
    both, at, found = (lax.all_gather(jnp.concatenate(lines), axis), 0, {})
    for k, line in zip(turns, lines):
        piece = both[:, at : at + len(line)].reshape(len(both), -1)
        found[k] = piece[:, : leaves[k].size].reshape(-1, *leaves[k].shape)
        at += len(line)
    numbers = iter(range(len(leaves)))
    return jax.tree.map(lambda _: found[next(numbers)], array)


def carried_in(array, axes, combine, identity):
    before = start = filled_with(array, identity)
    total = array
    for axis in reversed(axes):
        peers, mine = (lax.axis_size(axis), lax.axis_index(axis))
        pieces = collected_together(total, axis)
        inside, total = (start, start)
        for k in range(peers):
            passed = k < mine
            total = combine(total, jax.tree.map(lambda part: part[k], pieces))
            inside = jax.tree.map(lambda new, old: jnp.where(passed, new, old), total, inside)
        before = combine(inside, before)
    return before


def whole_of(array, axes, dim):
    for axis in reversed(axes):
        array = lax.all_gather(array, axis, axis=dim, tiled=True)
    return array


def in_order(parts, dim):
    lengths = list(parts.shape[1:])
    lengths[dim] *= parts.shape[0]
    return jnp.moveaxis(parts, 0, dim).reshape(lengths)


def copy_for_each(array, axis):
    peers = lax.axis_size(axis)
    return lax.all_to_all(
        jnp.broadcast_to(array[None], (peers, *array.shape)), axis, 0, 0, tiled=True
    )


def collect(array, axis, dim):
    return in_order(copy_for_each(array, axis), dim)


def rotate(source, positions, heads_here, factor):
    row_count, feat_width = source.shape
    head_dim = feat_width // heads_here
    half_dim = head_dim // 2
    values_f = source.astype(jnp.float32).reshape(row_count, heads_here, head_dim)
    inverse = 10000.0 ** (-jnp.arange(half_dim, dtype=jnp.float32) / half_dim)
    angles = positions[:, None] * inverse[None, :]
    cosine = jnp.cos(angles)[:, None, :]
    sine_part = jnp.sin(angles)[:, None, :]
    first_half = values_f[..., :half_dim]
    second_half = values_f[..., half_dim:]
    turned = jnp.concatenate(
        [
            first_half * cosine - second_half * sine_part,
            first_half * sine_part + second_half * cosine,
        ],
        axis=-1,
    )
    return (turned * factor).astype(jnp.bfloat16).reshape(row_count, feat_width)


def chain_states(earlier, later):
    return (earlier[0] * later[0], later[0][:, None, None] * earlier[1] + later[1])


def retention_half(queries, keys, values, gates, log_decay, out_weight):
    row_count, feat_width = queries.shape
    heads_here = log_decay.shape[1]
    head_dim = feat_width // heads_here
    block_count = row_count // BLOCK
    positions = (lax.axis_index(EP) * row_count + jnp.arange(row_count, dtype=jnp.int32)).astype(
        jnp.float32
    )
    rot_q = rotate(queries, positions, heads_here, 1.0)
    rot_k = rotate(keys, positions, heads_here, head_dim ** (-0.5))
    block_shape = (block_count, BLOCK, heads_here, head_dim)
    q_blocks = rot_q.reshape(block_shape)
    k_blocks = rot_k.reshape(block_shape)
    v_blocks = values.reshape(block_shape)
    cumulative = jnp.cumsum(log_decay.reshape(block_count, BLOCK, heads_here), axis=1)
    across = jnp.swapaxes(cumulative, 1, 2)
    spread = across[..., :, None] - across[..., None, :]
    causal = jnp.arange(BLOCK)[:, None] >= jnp.arange(BLOCK)[None, :]
    weights = jnp.where(causal, jnp.exp(jnp.where(causal, spread, 0.0)), 0.0)
    scores = jnp.einsum("nihd,njhd->nhij", q_blocks, k_blocks, preferred_element_type=jnp.float32)
    rounded = (scores * weights).astype(jnp.bfloat16)
    inside = jnp.einsum("nhij,njhd->nihd", rounded, v_blocks, preferred_element_type=jnp.float32)
    ending = cumulative[:, -1, :]
    k_scaled = k_blocks.astype(jnp.float32) * jnp.exp(ending[:, None, :] - cumulative)[..., None]
    updates = jnp.einsum(
        "njhd,njhe->nhde", k_scaled, v_blocks.astype(jnp.float32), precision=lax.Precision.HIGHEST
    )

    def advance(carry_state, member):
        return (jnp.exp(member[0])[:, None, None] * carry_state + member[1], carry_state)

    zero_state = jnp.zeros((heads_here, head_dim, head_dim), jnp.float32)
    local_end, before = lax.scan(advance, zero_state, (ending, updates))
    device_decay = jnp.exp(jnp.sum(ending, axis=0))
    incoming = carried_in(
        (device_decay, local_end), EP, chain_states, (jnp.ones_like(device_decay), zero_state)
    )
    leading = jnp.cumsum(ending, axis=0) - ending
    entering = before + jnp.exp(leading)[:, :, None, None] * incoming[1][None]
    carried = (
        jnp.einsum(
            "nihd,nhde->nihe",
            q_blocks.astype(jnp.float32),
            entering,
            precision=lax.Precision.HIGHEST,
        )
        * jnp.exp(cumulative)[..., None]
    )
    retained = (inside + carried).reshape(row_count, heads_here, head_dim)
    gate_f = gates.astype(jnp.float32).reshape(row_count, heads_here, head_dim)
    scaled = retained * lax.rsqrt(jnp.mean(retained * retained, axis=-1, keepdims=True) + 1e-05)
    head_out = (scaled * jax.nn.silu(gate_f)).astype(jnp.bfloat16).reshape(row_count, feat_width)
    projected = jnp.dot(whole_of(head_out, TP, 1), out_weight, preferred_element_type=jnp.float32)
    return projected.astype(jnp.bfloat16)


def expert_half(moe_rows, moe_gain, routes, route_weights, gate_proj, up_proj, down_proj):
    row_count, feat_width = moe_rows.shape
    experts = lax.axis_size(EP)
    capacity = 2 * row_count // experts
    as_float = moe_rows.astype(jnp.float32)
    normed = (
        as_float
        * lax.rsqrt(jnp.mean(as_float * as_float, axis=-1, keepdims=True) + 1e-06)
        * moe_gain.astype(jnp.float32)
    ).astype(jnp.bfloat16)
    flat_ids = routes.reshape(-1)
    onehot = (flat_ids[:, None] == jnp.arange(experts, dtype=jnp.int32)[None, :]).astype(jnp.int32)
    slot_rank = jnp.sum((jnp.cumsum(onehot, axis=0) - onehot) * onehot, axis=1)
    target = flat_ids * capacity + slot_rank
    source_row = (
        jnp.zeros((experts * capacity,), jnp.int32)
        .at[target]
        .set(jnp.arange(2 * row_count, dtype=jnp.int32) // 2)
    )
    outgoing = normed[source_row].reshape(experts, capacity, feat_width)
    w_gate = gate_proj[0]
    w_up = up_proj[0]
    w_down = down_proj[0]
    share_size = capacity // lax.axis_size(TP)
    own_share = lax.dynamic_slice_in_dim(outgoing, lax.axis_index(TP) * share_size, share_size, 1)
    arrived_share = lax.all_to_all(own_share, EP, split_axis=0, concat_axis=0, tiled=True)
    arrived = collect(arrived_share, TP, 1)
    gate_part = jnp.einsum("scd,df->scf", arrived, w_gate, preferred_element_type=jnp.float32)
    up_part = jnp.einsum("scd,df->scf", arrived, w_up, preferred_element_type=jnp.float32)
    hidden = (jax.nn.silu(gate_part) * up_part).astype(jnp.bfloat16)
    expert_out = jnp.einsum(
        "scf,fd->scd",
        lax.all_gather(hidden, TP, axis=2, tiled=True),
        w_down,
        preferred_element_type=jnp.float32,
    ).astype(jnp.bfloat16)
    returned = lax.all_to_all(expert_out, EP, split_axis=0, concat_axis=0, tiled=True)
    picked = returned.reshape(experts * capacity, -1)[target].reshape(row_count, 2, -1)
    return jnp.sum(picked.astype(jnp.float32) * route_weights[:, :, None], axis=1).astype(
        jnp.bfloat16
    )


def on_device(
    queries,
    keys,
    values,
    gates,
    log_decay,
    out_weight,
    moe_rows,
    moe_gain,
    routes,
    route_weights,
    gate_proj,
    up_proj,
    down_proj,
):
    mixer_out = retention_half(queries, keys, values, gates, log_decay, out_weight)
    moe_out = expert_half(moe_rows, moe_gain, routes, route_weights, gate_proj, up_proj, down_proj)
    return (mixer_out, moe_out)


def solution(mesh):
    torus = Mesh(mesh.devices.reshape(16, 2, 4, 4), ("ep_0", "ep_1", "tp_0", "tp_1"))
    return jax.shard_map(
        on_device,
        mesh=torus,
        in_specs=(
            P(EP, TP),
            P(EP, TP),
            P(EP, TP),
            P(EP, TP),
            P(EP, TP),
            P(None, TP),
            P(EP, None),
            P(),
            P(EP, None),
            P(EP, None),
            P(EP, None, TP),
            P(EP, None, TP),
            P(EP, None, TP),
        ),
        out_specs=(P(EP, TP), P(EP, TP)),
        check_vma=False,
    )
```

profile of v0, /device:TPU:1, one launch (start us, length us, event | category | flops | bytes accessed | tf_op | source)
XLA Modules:
  0.0 249.1 jit_solution(12538296000440214369)
XLA Ops:
  7.2 1.0 copy.44
  8.4 0.7 broadcast_multiply_fusion
  9.1 1.2 reduce-window.18
  11.0 2.4 scatter_custom_fusion
  13.5 0.7 convert_element_type.89
  14.2 1.5 fusion
  16.0 3.3 %gather_fusion = bf16[512,2048]{1,0:T(8,128)(2,1)} fusion(bf16[256,2048]{1,0:T(8,128)(2,1)S(1)} %fusion.2, s32[1024]{0:T(1024)S(1)} %pad_clamp_fusion.1), kind=kCustom, calls=%fused_computation | custom fusion | bytes 4196352 | tf_op jit(solution)/shard_map/gather | solution.py:173
  19.4 1.5 constant_dynamic-slice_fusion.1
  20.9 0.5 broadcast.370
  21.4 1.4 reduce.10
  22.8 0.7 reshape.656
  23.5 16.7 %all-to-all-start = ((bf16[32,2,1024]{2,1,0:T(2,128)(2,1)}), bf16[32,2,1024]{2,1,0:T(2,128)(2,1)S(1)}, u32[]{:S(2)}, u32[]{:S(2)}) async-start(bf16[32,2,1024]{2,1,0:T(2,128)(2,1)} %reshape.656), calls=%async_computation | async-start | bytes 262144 | tf_op jit(solution)/shard_map/all_to_all | solution.py:179
  40.7 0.6 slice_reduce_fusion.1
  41.4 0.6 fusion.34
  42.2 0.6 fusion.80
  43.1 2.4 while.13
  43.1 0.6 fusion.88
  43.7 0.6 bitcast_add_fusion.2
  44.3 0.6 fusion.88
  44.9 0.6 bitcast_add_fusion.2
  46.2 0.5 pad_bitcast_fusion.1
  46.7 9.4 %all-to-all-done = bf16[32,2,1024]{2,1,0:T(2,128)(2,1)S(1)} async-done(((bf16[32,2,1024]{2,1,0:T(2,128)(2,1)}), bf16[32,2,1024]{2,1,0:T(2,128)(2,1)S(1)}, u32[]{:S(2)}, u32[]{:S(2)}) %all-to-all-start) | async-done | bytes 131104 | tf_op jit(solution)/shard_map/all_to_all | solution.py:179
  56.3 1.6 broadcast_in_dim.33
  57.9 6.8 %all-to-all-start.1 = ((bf16[16,32,1,2048]{3,1,2,0:T(8,128)(2,1)}), bf16[16,32,1,2048]{3,1,2,0:T(8,128)(2,1)S(1)}, u32[]{:S(2)}, u32[]{:S(2)}) async-start(bf16[16,32,1,2048]{3,1,2,0:T(8,128)(2,1)} %broadcast_in_dim.33), calls=%async_computation.1 | async-start | bytes 4194304 | tf_op jit(solution)/shard_map/all_to_all | solution.py:64
  64.8 3.4 %all-gather.2 = f32[2,129,128]{2,1,0:T(8,128)S(1)} all-gather(f32[1,129,128]{2,1,0:T(8,128)S(1)} %maximum_bitcast_fusion), channel_id=2, replica_groups=mesh['ep_0'=16,'ep_1'=2,'tp_0'=4,'tp_1'=4] {'ep_1'}, dimensions={0}, use_global_device_ids=true | all-gather | bytes 198144 | tf_op jit(solution)/shard_map/all_gather | solution.py:26
  68.2 0.6 fusion.79
  70.7 0.7 fusion.66
  71.4 0.6 maximum_bitcast_fusion.1
  72.1 20.5 %all-to-all-done.1 = bf16[16,32,1,2048]{3,1,2,0:T(8,128)(2,1)S(1)} async-done(((bf16[16,32,1,2048]{3,1,2,0:T(8,128)(2,1)}), bf16[16,32,1,2048]{3,1,2,0:T(8,128)(2,1)S(1)}, u32[]{:S(2)}, u32[]{:S(2)}) %all-to-all-start.1) | async-done | bytes 2097184 | tf_op jit(solution)/shard_map/all_to_all | solution.py:64
  92.6 0.7 fusion.5
  93.3 0.5 copy-done.12
  93.8 1.4 fusion.10
  95.3 0.9 reduce-window.14
  96.8 0.6 fusion.72
  97.5 26.1 %all-gather.12.cloned.1.call-done = f32[16,129,128]{2,1,0:T(8,128)} async-done(((f32[1,129,128]{2,1,0:T(8,128)}), f32[16,129,128]{2,1,0:T(8,128)}) %all-gather.12.cloned.1.call-update) | async-done | bytes 1056784 | tf_op jit(solution)/shard_map/all_gather | solution.py:26
  123.6 0.8 slice.250
  124.4 0.6 fusion.78
  125.7 11.5 %fusion.57 = f32[128,128]{1,0:T(8,128)S(1)} fusion(f32[16,129,128]{2,1,0:T(8,128)} %all-gather.12.cloned.1.call-done, f32[2,129,128]{2,1,0:T(8,128)S(1)} %all-gather.2, f32[]{:T(128)} %bitcast.46, f32[]{:T(128)} %bitcast.45, f32[]{:T(128)} %bitcast.44, f32[]{:T(128)} %bitcast.43, f32[]{:T(128)} %bitcast.42, f32[]{:T(128)} %bitcast.41, f32[]{:T(128)} %bitcast.40, ...), kind=kLoop, calls=%fused_computation.81 | loop fusion | flops 884736 | bytes 1245278 | tf_op jit(solution)/shard_map/mul | solution.py:136
  137.2 1.2 fusion.14
  139.0 10.0 %all_gather.25 = bf16[256,512]{1,0:T(8,128)(2,1)} all-gather(bf16[256,128]{1,0:T(8,128)(2,1)S(1)} %fusion.50), channel_id=1, replica_groups=mesh['ep_0'=16,'ep_1'=2,'tp_0'=4,'tp_1'=4] {'tp_1'}, dimensions={1}, use_global_device_ids=true | all-gather | bytes 327680 | tf_op jit(solution)/shard_map/all_gather | solution.py:52
  149.0 56.0 %all-gather.10.cloned.1.call-done = bf16[32,16,4096]{2,0,1:T(8,128)(2,1)} async-done(((bf16[32,16,256]{2,0,1:T(8,128)(2,1)}), bf16[32,16,4096]{2,0,1:T(8,128)(2,1)}) %all-gather.10.cloned.1.call-update) | async-done | bytes 4194320 | tf_op jit(solution)/shard_map/all_gather | solution.py:186
  205.0 3.4 %fusion.16 = bf16[32,16,128]{2,0,1:T(8,128)(2,1)S(1)} fusion(bf16[32,16,4096]{2,0,1:T(8,128)(2,1)} %all-gather.10.cloned.1.call-done, bf16[1,4096,128]{2,1,0:T(8,128)(2,1)S(1)} %copy-done.13), kind=kOutput, calls=%fused_computation.25 | convolution fusion | flops 536870912 | bytes 5373952 | tf_op jit(solution)/shard_map/scf,fd->scd/dot_general | solution.py:184
  208.4 0.7 copy.58
  209.1 14.4 %all-to-all-start.2 = ((bf16[32,16,128]{2,1,0:T(8,128)(2,1)}), bf16[32,16,128]{2,1,0:T(8,128)(2,1)S(1)}, u32[]{:S(2)}, u32[]{:S(2)}) async-start(bf16[32,16,128]{2,1,0:T(8,128)(2,1)} %copy.58), calls=%async_computation.2 | async-start | bytes 262144 | tf_op jit(solution)/shard_map/all_to_all | solution.py:190
  223.6 14.2 %all-gather.8.cloned.1.call-done = bf16[256,2048]{1,0:T(8,128)(2,1)} async-done(((bf16[256,512]{1,0:T(8,128)(2,1)}), bf16[256,2048]{1,0:T(8,128)(2,1)}) %all-gather.8.cloned.1.call-update) | async-done | bytes 1048592 | tf_op jit(solution)/shard_map/all_gather | solution.py:52
  237.8 2.3 convolution_convert_fusion
  240.1 1.3 gather_fusion.1
  241.5 1.1 fusion.20
  (72 shorter events, 3.4 us)
Async XLA Ops:
  7.2 85.4 %copy-start = (bf16[1,2048,256]{2,1,0:T(8,128)(2,1)S(1)}, bf16[1,2048,256]{2,1,0:T(8,128)(2,1)}, u32[]{:S(2)}) copy-start(bf16[1,2048,256]{2,1,0:T(8,128)(2,1)} %param.25) | copy-start | bytes 3145732
  7.2 8.5 %copy-start.1 = (bf16[256,2048]{1,0:T(8,128)(2,1)S(1)}, bf16[256,2048]{1,0:T(8,128)(2,1)}, u32[]{:S(2)}) copy-start(bf16[256,2048]{1,0:T(8,128)(2,1)} %param.21) | copy-start | bytes 3145732
  16.0 24.3 %copy-start.10 = (f32[256,1]{0,1:T(1,128)S(1)}, f32[256,1]{0,1:T(1,128)}, u32[]{:S(2)}) copy-start(f32[256,1]{0,1:T(1,128)} %param.19) | copy-start | bytes 3076
  16.0 25.4 %copy-start.4 = (bf16[256,128]{1,0:T(8,128)(2,1)S(1)}, bf16[256,128]{1,0:T(8,128)(2,1)}, u32[]{:S(2)}) copy-start(bf16[256,128]{1,0:T(8,128)(2,1)} %param.16) | copy-start | bytes 196612
  16.0 25.4 %copy-start.5 = (bf16[256,128]{1,0:T(8,128)(2,1)S(1)}, bf16[256,128]{1,0:T(8,128)(2,1)}, u32[]{:S(2)}) copy-start(bf16[256,128]{1,0:T(8,128)(2,1)} %param.15) | copy-start | bytes 196612
  19.4 23.4 %copy-start.6 = (bf16[256,128]{1,0:T(8,128)(2,1)S(1)}, bf16[256,128]{1,0:T(8,128)(2,1)}, u32[]{:S(2)}) copy-start(bf16[256,128]{1,0:T(8,128)(2,1)} %param.17) | copy-start | bytes 196612
  23.5 32.6 %all-to-all-start = ((bf16[32,2,1024]{2,1,0:T(2,128)(2,1)}), bf16[32,2,1024]{2,1,0:T(2,128)(2,1)S(1)}, u32[]{:S(2)}, u32[]{:S(2)}) async-start(bf16[32,2,1024]{2,1,0:T(2,128)(2,1)} %reshape.656), calls=%async_computation | async-start | bytes 262144 | tf_op jit(solution)/shard_map/all_to_all | solution.py:179
  45.5 1.2 copy-start.3
  45.5 12.4 %copy-start.9 = (f32[2,1]{0,1:T(1,128)}, f32[2,1]{0,1:T(1,128)S(1)}, u32[]{:S(2)}) copy-start(f32[2,1]{0,1:T(1,128)S(1)} %get-tuple-element.178) | copy-start | bytes 28
  57.9 6.8 %copy-start.11 = (f32[1,128]{1,0:T(1,128)S(1)}, f32[1,128]{1,0:T(1,128)}, u32[]{:S(2)}) copy-start(f32[1,128]{1,0:T(1,128)} %pad_bitcast_fusion.1) | copy-start | bytes 1540
  57.9 34.6 %all-to-all-start.1 = ((bf16[16,32,1,2048]{3,1,2,0:T(8,128)(2,1)}), bf16[16,32,1,2048]{3,1,2,0:T(8,128)(2,1)S(1)}, u32[]{:S(2)}, u32[]{:S(2)}) async-start(bf16[16,32,1,2048]{3,1,2,0:T(8,128)(2,1)} %broadcast_in_dim.33), calls=%async_computation.1 | async-start | bytes 4194304 | tf_op jit(solution)/shard_map/all_to_all | solution.py:64
  64.7 58.9 %all-gather.12.cloned.1.call-start = ((), (), s32[]{:S(2)}) async-start(), calls=%async_computation.5 | async-start | bytes 1183744 | tf_op jit(solution)/shard_map/all_gather | solution.py:26
  72.0 132.9 %all-gather.10.cloned.1.call-start = ((), (), s32[]{:S(2)}) async-start(), calls=%async_computation.4 | async-start | bytes 4456448 | tf_op jit(solution)/shard_map/all_gather | solution.py:186
  92.6 1.2 copy-start.12
  95.2 43.6 %copy-start.7 = (bf16[256,128]{1,0:T(8,128)(2,1)S(1)}, bf16[256,128]{1,0:T(8,128)(2,1)}, u32[]{:S(2)}) copy-start(bf16[256,128]{1,0:T(8,128)(2,1)} %param.18) | copy-start | bytes 196612
  95.2 109.7 %copy-start.13 = (bf16[1,4096,128]{2,1,0:T(8,128)(2,1)S(1)}, bf16[1,4096,128]{2,1,0:T(8,128)(2,1)}, u32[]{:S(2)}) copy-start(bf16[1,4096,128]{2,1,0:T(8,128)(2,1)} %param.27) | copy-start | bytes 3145732
  95.2 142.6 %all-gather.8.cloned.1.call-start = ((), (), s32[]{:S(2)}) async-start(), calls=%async_computation.3 | async-start | bytes 1310720 | tf_op jit(solution)/shard_map/all_gather | solution.py:52
  149.0 74.5 %copy-start.8 = (f32[256,2]{0,1:T(2,128)S(1)}, f32[256,2]{0,1:T(2,128)}, u32[]{:S(2)}) copy-start(f32[256,2]{0,1:T(2,128)} %param.24) | copy-start | bytes 6148
  149.0 88.9 %copy-start.2 = (bf16[2048,128]{1,0:T(8,128)(2,1)S(1)}, bf16[2048,128]{1,0:T(8,128)(2,1)}, u32[]{:S(2)}) copy-start(bf16[2048,128]{1,0:T(8,128)(2,1)} %param.20) | copy-start | bytes 1572868
  209.1 31.0 %all-to-all-start.2 = ((bf16[32,16,128]{2,1,0:T(8,128)(2,1)}), bf16[32,16,128]{2,1,0:T(8,128)(2,1)S(1)}, u32[]{:S(2)}, u32[]{:S(2)}) async-start(bf16[32,16,128]{2,1,0:T(8,128)(2,1)} %copy.58), calls=%async_computation.2 | async-start | bytes 262144 | tf_op jit(solution)/shard_map/all_to_all | solution.py:190
Sparse Core Ops, SparseCore 0:
  72.1 51.4 all-gather.11
  126.6 78.3 all-gather.9
  207.1 30.7 all-gather.7
where the time goes:
time: 251 us; the launch traced here: 249 us
  waiting for transfers between devices  126 us (50%)
  starting transfers between devices  38 us (15%)
  other arithmetic  24.8 us (10%)
  local copies, waits for them, and re-layouts  18.7 us (7%)
  between operations  18 us (7%)
  blocking collectives  13.4 us (5%)
  matrix products  9.84 us (4%)
    all_gather x1, waiting for transfers between devices, expert_half(): lax.all_gather(hidden, TP, axis=2, tiled=True)  56 us
    all_gather x1, waiting for transfers between devices, collected_together(): both, at, found = (lax.all_gather(jnp.concatenate(lines), axis), 0, {})  26.1 us
    all_to_all x1, waiting for transfers between devices, copy_for_each(): lax.all_to_all(jnp.broadcast_to(array[None], (peers, *array.shape)), axis...  20.5 us
    all_to_all x1, starting transfers between devices, expert_half(): lax.all_to_all(own_share, EP, split_axis=0, concat_axis=0, tiled=True)  16.7 us
    all_to_all x1, starting transfers between devices, expert_half(): lax.all_to_all(expert_out, EP, split_axis=0, concat_axis=0, tiled=True)  14.4 us
    all_gather x1, waiting for transfers between devices, whole_of(): array = lax.all_gather(array, axis, axis=dim, tiled=True)  14.2 us
    mul x1, other arithmetic, retention_half(): entering = before + jnp.exp(leading)[:, :, None, None] * incoming[1][None]  11.5 us
    all_gather x1, blocking collectives, whole_of(): array = lax.all_gather(array, axis, axis=dim, tiled=True)  9.98 us
  transfers between devices with their start and end apart: 6, of which 5 were waited for; matrix products, arithmetic and copies ran while one was open for 13% of the time, Pallas kernels for 0%

commit v1 on v0

v1 whole, which is shorter than its diff:
```python
import jax
import jax.numpy as jnp
import numpy as np
from jax import lax
from jax.experimental import pallas as pl
from jax.experimental.pallas import tpu as pltpu
from jax.sharding import Mesh
from jax.sharding import PartitionSpec as P

MESH = pl.DeviceIdType.MESH
F32 = jnp.float32
BF16 = jnp.bfloat16
Z, C, Y, X = 16, 2, 4, 4
E = Z * C
T = Y * X
ROWS = 256
SLOTS = 2 * ROWS
CAP = SLOTS // E
D = 2048
W = 128
BLOCK = 128
EP = ("ep_0", "ep_1")
TP = ("tp_0", "tp_1")


def mm(a, b, ca=1, cb=0):
    return lax.dot_general(a, b, (((ca,), (cb,)), ((), ())), preferred_element_type=F32)


def parts_of(a, count):
    found = []
    for k in range(count):
        piece = a.astype(BF16)
        found.append(piece)
        if k + 1 < count:
            a = a - piece.astype(F32)
    return found


def silu(v):
    return v / (1.0 + jnp.exp(-v))


class Copies:
    def __init__(self, send, recv, place):
        self.send, self.recv, self.place = send, recv, place
        self.count = 0
        self.sent = []

    def ids(self, n):
        first = self.count
        self.count += n
        return first

    def make(self, k, src, dst, dev):
        return pltpu.make_async_remote_copy(
            src_ref=src,
            dst_ref=dst,
            send_sem=self.send.at[k],
            recv_sem=self.recv.at[k],
            device_id=dev,
            device_id_type=MESH,
        )

    def start(self, k, src, dst, dev):
        copy = self.make(k, src, dst, dev)
        copy.start()
        self.sent.append(copy)

    def landed(self, k, region, dev):
        self.make(k, region, region, dev).wait_recv()

    def drain(self):
        for copy in self.sent:
            copy.wait_send()
        self.sent = []


class Spread:
    def __init__(self, copies, buf, h0, n, first):
        self.c, self.buf, self.h0, self.n, self.first = copies, buf, h0, n, first
        self.k = copies.ids(20)

    def offset(self, dp, dq):
        y, x = self.c.place
        dy, dx = (dq, dp) if self.first == "x" else (dp, dq)
        return lax.rem(y + dy + Y, Y), lax.rem(x + dx + X, X)

    def ref(self, dp, dq, part=None):
        y, x = self.offset(dp, dq)
        block = y * X + x
        if part is None:
            return self.buf.at[block, pl.ds(self.h0, self.n)]
        half = self.n // 2
        return self.buf.at[block, pl.ds(self.h0 + part * half, half)]

    def dev(self, dp, dq):
        y, x = self.offset(dp, dq)
        return {"tp_0": y, "tp_1": x}

    def go(self, k, block, to, part=None):
        ref = self.ref(*block, part)
        self.c.start(self.k + k, ref, ref, self.dev(*to))

    def got(self, k, block, part=None):
        self.c.landed(self.k + k, self.ref(*block, part), self.dev(0, 1))

    def turn(self, j):
        return {0: 0, -1: 1, 1: 2, 2: 3}[j]

    def first_own(self):
        self.go(0, (0, 0), (1, 0))
        self.go(1, (0, 0), (-1, 0))

    def across(self, j):
        base = 4 + 4 * self.turn(j)
        self.go(base, (j, 0), (0, 1))
        self.go(base + 1, (j, 0), (0, -1))

    def first_left(self):
        self.got(0, (-1, 0))
        self.go(2, (-1, 0), (1, 0), 0)

    def first_right(self):
        self.got(1, (1, 0))
        self.go(3, (1, 0), (-1, 0), 1)

    def first_far(self):
        self.got(2, (2, 0), 0)
        self.got(3, (2, 0), 1)

    def relay(self, j):
        base = 4 + 4 * self.turn(j)
        self.got(base, (j, -1))
        self.go(base + 2, (j, -1), (0, 1), 0)
        self.got(base + 1, (j, 1))
        self.go(base + 3, (j, 1), (0, -1), 1)

    def far(self, j):
        base = 4 + 4 * self.turn(j)
        self.got(base + 2, (j, 2), 0)
        self.got(base + 3, (j, 2), 1)


def both(pair, step, *args):
    for half in pair:
        getattr(half, step)(*args)


def kernel(
    q_ref, k_ref, v_ref, g_ref, ld_ref, wo_hbm, rows_ref, gain_ref, routes_ref, rw_ref,
    wg_hbm, wu_hbm, wd_hbm, cr_ref, sr_ref, cb_ref, sb_ref,
    mix_ref, moe_ref,
    wg, wu, wo, wa, wb, oh, snd, rbuf, acc, ha, hb, pa, pb, ra, rb, eo, ret,
    sts, str_, sto, sti, ins, rotq, cum, upd, ho,
    lsem, send, recv, zsem,
):
    z, c = lax.axis_index("ep_0"), lax.axis_index("ep_1")
    y, x = lax.axis_index("tp_0"), lax.axis_index("tp_1")
    e = z * C + c
    t = y * X + x
    copies = Copies(send, recv, (y, x))

    barrier = pltpu.get_barrier_semaphore()

    def ring_dev(d):
        j = lax.rem(e + d, E)
        return j, {"ep_0": j // C, "ep_1": lax.rem(j, C)}

    def greet(d, _):
        pl.semaphore_signal(barrier, inc=1, device_id=ring_dev(d)[1], device_id_type=MESH)
        return _

    lax.fori_loop(1, E, greet, 0)
    for s in range(1, 4):
        pl.semaphore_signal(
            barrier, inc=1, device_id={"tp_0": lax.rem(y + s, Y)}, device_id_type=MESH
        )
        pl.semaphore_signal(
            barrier, inc=1, device_id={"tp_1": lax.rem(x + s, X)}, device_id_type=MESH
        )

    wd_rows = wd_hbm
    local = [
        pltpu.make_async_copy(wg_hbm, wg, lsem.at[0]),
        pltpu.make_async_copy(wu_hbm, wu, lsem.at[1]),
        pltpu.make_async_copy(wd_rows.at[y, :, 0], wa.at[y], lsem.at[2]),
        pltpu.make_async_copy(wd_rows.at[:, x, 1], wb.at[x], lsem.at[3]),
        pltpu.make_async_copy(wo_hbm, wo, lsem.at[4]),
    ]
    for copy in local:
        copy.start()

    slot_id = lax.broadcasted_iota(jnp.int32, (SLOTS, ROWS), 0)
    expert_of = slot_id // CAP
    place_of = (slot_id - expert_of * CAP).astype(F32)
    named = [routes_ref[k : k + 1, :] == expert_of for k in range(2)]
    either = jnp.logical_or(named[0], named[1])
    before = (
        lax.broadcasted_iota(jnp.int32, (ROWS, ROWS), 0)
        < lax.broadcasted_iota(jnp.int32, (ROWS, ROWS), 1)
    )
    rank = mm(either.astype(F32).astype(BF16), before.astype(F32).astype(BF16))
    here = rank == place_of
    for k in range(2):
        oh[k] = jnp.logical_and(named[k], here).astype(F32).astype(BF16)

    lanes = pl.ds(pl.multiple_of(t * W, W), W)

    def squares(r, _):
        rows = pl.ds(pl.multiple_of(r * 64, 64), 64)
        full = rows_ref[rows, :].astype(F32)
        mean = jnp.sum(full * full, axis=-1, keepdims=True) * (1.0 / D)
        mine = rows_ref[rows, lanes].astype(F32)
        normed = mine * lax.rsqrt(mean + 1e-06) * gain_ref[:, lanes].astype(F32)
        rotq[rows, :] = normed.astype(BF16)
        return _

    lax.fori_loop(0, ROWS // 64, squares, 0)
    normed = rotq[...]
    picked = mm(oh[0] + oh[1], normed)
    snd[...] = picked.astype(BF16)
    mine_at = pl.ds(pl.multiple_of(e * CAP, CAP), CAP)
    rbuf[t, mine_at, :] = snd[mine_at, :]

    pl.semaphore_wait(barrier, E - 1 + 6)

    def far_first(i):
        half = (i + 1) // 2
        return E // 2 + half * (1 - 2 * lax.rem(i, 2))

    def dispatch(i, _):
        j, dev = ring_dev(far_first(i))
        pltpu.make_async_remote_copy(
            src_ref=snd.at[pl.ds(pl.multiple_of(j * CAP, CAP), CAP)],
            dst_ref=rbuf.at[t, mine_at],
            send_sem=zsem.at[0],
            recv_sem=zsem.at[1],
            device_id=dev,
            device_id_type=MESH,
        ).start()
        return _

    lax.fori_loop(0, E - 1, dispatch, 0)

    wk = copies.ids(6)
    for s in (2, 1, 3):
        yy, xx = lax.rem(y + s, Y), lax.rem(x + s, X)
        copies.start(wk + s - 1, wd_rows.at[yy, :, 0], wa.at[y], {"tp_0": yy})
        copies.start(wk + 2 + s, wd_rows.at[:, xx, 1], wb.at[x], {"tp_1": xx})

    cb, sb = cb_ref[e], sb_ref[e]
    cos = cb * cr_ref[...] - sb * sr_ref[...]

    def signed(first, second):
        lane = lax.broadcasted_iota(jnp.int32, first.shape, 1)
        return jnp.where(lane < W // 2, -first, second)

    sin = sb * cr_ref[...] + cb * sr_ref[...]
    sin = signed(sin, sin)

    def turned(ref):
        full = ref[...].astype(F32)
        return full * cos + pltpu.roll(full, W // 2, 1) * sin

    rq = turned(q_ref).astype(BF16)
    rotq[...] = rq
    rk = (turned(k_ref) * (W**-0.5)).astype(BF16)
    row_i = lax.broadcasted_iota(jnp.int32, (BLOCK, BLOCK), 0)
    col_i = lax.broadcasted_iota(jnp.int32, (BLOCK, BLOCK), 1)
    causal = row_i >= col_i
    tri = causal.astype(F32).astype(BF16)
    ends = []
    for b in range(2):
        rows = slice(b * BLOCK, (b + 1) * BLOCK)
        decay = jnp.broadcast_to(ld_ref[b : b + 1, :], (BLOCK, BLOCK))
        column = jnp.zeros((BLOCK, BLOCK), F32)
        line = jnp.zeros((BLOCK, BLOCK), F32)
        for piece in parts_of(decay, 3):
            column = column + mm(tri, piece, 1, 1)
            line = line + mm(piece, tri, 1, 1)
        spread = column - line
        factor = jnp.where(causal, jnp.exp(jnp.where(causal, spread, 0.0)), 0.0)
        weights = (mm(rq[rows], rk[rows], 1, 1) * factor).astype(BF16)
        values = v_ref[rows, :]
        cum[rows, :] = column
        end = column[BLOCK - 1 : BLOCK, :]
        ends.append(end)
        scaled = rk[rows].astype(F32) * jnp.exp(end - column)
        high, low = parts_of(scaled, 2)
        upd[b] = mm(high, values, 0, 0) + mm(low, values, 0, 0)
        acc[rows, 0:W] = mm(weights, values)
    whole = jnp.exp(ends[1]) * upd[0] + upd[1]
    total = ends[0] + ends[1]
    for s in range(Z):
        sts[s, 0:8, :] = whole[s * 8 : (s + 1) * 8, :]
        sts[s, 8:9, :] = total
    upd[1] = jnp.broadcast_to(jnp.exp(ends[0]), (BLOCK, W))
    inside = acc[0:ROWS, 0:W]
    ins[...] = inside

    owner = c == lax.rem(z, C)
    str_[e] = sts[z]

    def give(i, carry):
        s = lax.rem(z + i, Z)

        @pl.when(jnp.logical_or(i > 0, jnp.logical_not(owner)))
        def _():
            pltpu.make_async_remote_copy(
                src_ref=sts.at[s],
                dst_ref=str_.at[e],
                send_sem=zsem.at[4],
                recv_sem=zsem.at[5],
                device_id={"ep_0": s, "ep_1": lax.rem(s, C)},
                device_id_type=MESH,
            ).start()

        return carry

    lax.fori_loop(0, Z, give, 0)

    def z_all(buf, sem, kind):
        part = buf.at[pl.ds(0, (E - 1) * CAP)]
        copy = pltpu.make_async_remote_copy(
            src_ref=part, dst_ref=part, send_sem=zsem.at[sem], recv_sem=zsem.at[sem],
            device_id={"tp_1": lax.rem(x + 1, X)}, device_id_type=MESH,
        )
        if kind == "recv":
            copy.wait_recv()
        else:
            copy.wait_send()

    z_all(rbuf.at[t], 1, "recv")
    moe = (Spread(copies, rbuf, 0, ROWS, "x"), Spread(copies, rbuf, ROWS, ROWS, "y"))
    both(moe, "first_own")
    both(moe, "across", 0)

    def state_all(buf, count, sem, kind):
        part = buf.at[pl.ds(0, count)]
        copy = pltpu.make_async_remote_copy(
            src_ref=part, dst_ref=part, send_sem=zsem.at[sem], recv_sem=zsem.at[sem],
            device_id={"tp_1": lax.rem(x + 1, X)}, device_id_type=MESH,
        )
        if kind == "recv":
            copy.wait_recv()
        else:
            copy.wait_send()

    @pl.when(owner)
    def _():
        state_all(str_, E - 1, 5, "recv")
        current = jnp.zeros((8, W), F32)
        for j in range(E):
            sto[j] = current
            if j + 1 < E:
                current = jnp.exp(str_[j, 8:9, :]) * current + str_[j, 0:8, :]
        sti[z] = sto[e]

        def back(i, _):
            j, dev = ring_dev(far_first(i))
            pltpu.make_async_remote_copy(
                src_ref=sto.at[j],
                dst_ref=sti.at[z],
                send_sem=zsem.at[6],
                recv_sem=zsem.at[7],
                device_id=dev,
                device_id_type=MESH,
            ).start()
            return _

        lax.fori_loop(0, E - 1, back, 0)

    both(moe, "first_left")
    both(moe, "across", -1)
    both(moe, "first_right")
    both(moe, "across", 1)
    both(moe, "relay", 0)
    both(moe, "first_far")
    both(moe, "across", 2)

    local[0].wait()
    local[1].wait()

    def gather_group(half, dq, fresh):
        rows = pl.ds(half.h0, half.n)
        blocks, left = [], []
        for k in range(4):
            yy, xx = half.offset(k, dq)
            blocks.append(yy * X + xx)
        left = jnp.concatenate([rbuf[b, rows, :] for b in blocks], axis=1)
        for at, weight in ((0, wg), (256, wu)):
            right = jnp.concatenate(
                [weight[pl.ds(pl.multiple_of(b * W, W), W), :] for b in blocks], axis=0
            )
            product = mm(left, right)
            if fresh:
                acc[rows, at : at + 256] = product
            else:
                acc[rows, at : at + 256] += product

    for half in moe:
        gather_group(half, 0, True)

    @pl.when(owner)
    def _():
        state_all(sti, Z - 1, 7, "recv")

    @pl.when(jnp.logical_not(owner))
    def _():
        state_all(sti, Z, 7, "recv")

    entering = sti[...].reshape(W, W)
    for b in range(2):
        rows = slice(b * BLOCK, (b + 1) * BLOCK)
        high, low = parts_of(entering, 2)
        query = rotq[rows, :]
        carried = (mm(query, high) + mm(query, low)) * jnp.exp(cum[rows, :])
        retained = ins[rows, :] + carried
        mean = jnp.sum(retained * retained, axis=-1, keepdims=True) * (1.0 / W)
        gate = g_ref[rows, :].astype(F32)
        ho[t, rows, :] = (retained * lax.rsqrt(mean + 1e-05) * silu(gate)).astype(BF16)
        entering = upd[1] * entering + upd[0]
    mix = (Spread(copies, ho, 0, BLOCK, "x"), Spread(copies, ho, BLOCK, BLOCK, "y"))
    both(mix, "first_own")
    both(mix, "across", 0)

    both(moe, "relay", -1)
    both(moe, "relay", 1)
    both(moe, "relay", 2)
    for half in moe:
        gather_group(half, -1, False)
        gather_group(half, 1, False)
    for j in (0, -1, 1, 2):
        both(moe, "far", j)
    for half in moe:
        gather_group(half, 2, False)

    hidden = (silu(acc[:, 0:256]) * acc[:, 256:512]).astype(BF16)
    ha[x] = hidden[:, 0:W]
    hb[y] = hidden[:, W : 2 * W]

    hk = copies.ids(8)

    def hop(k, axis, buf, block, to, part=None):
        me, size = (x, X) if axis == "tp_1" else (y, Y)
        ref = buf.at[lax.rem(me + block + size, size)]
        if part is not None:
            ref = ref.at[pl.ds(part * ROWS, ROWS)]
        return k, ref, {axis: lax.rem(me + to + size, size)}

    hsides = (("tp_1", ha, hk), ("tp_0", hb, hk + 4))
    for axis, buf, k in hsides:
        for n, to in ((0, 1), (1, -1)):
            kk, ref, dev = hop(k + n, axis, buf, 0, to)
            copies.start(kk, ref, ref, dev)

    both(mix, "first_left")
    both(mix, "across", -1)
    both(mix, "first_right")
    both(mix, "across", 1)

    for n, frm, part in ((0, -1, 0), (1, 1, 1)):
        for axis, buf, k in hsides:
            kk, ref, dev = hop(k + n, axis, buf, frm, 1)
            copies.landed(kk, ref, dev)
            kk, ref, dev = hop(k + 2 + n, axis, buf, frm, -frm, part)
            copies.start(kk, ref, ref, dev)

    both(mix, "relay", 0)
    both(mix, "first_far")
    both(mix, "across", 2)

    for axis, buf, k in hsides:
        for n in range(2):
            kk, ref, dev = hop(k + 2 + n, axis, buf, 2, 1, n)
            copies.landed(kk, ref, dev)

    local[2].wait()
    local[3].wait()
    for s in range(1, 4):
        copies.landed(wk + s - 1, wa.at[lax.rem(y + Y - s, Y)], {"tp_0": lax.rem(y + s, Y)})
        copies.landed(wk + 2 + s, wb.at[lax.rem(x + X - s, X)], {"tp_1": lax.rem(x + s, X)})

    left_a = jnp.concatenate([ha[k] for k in range(X)], axis=1)
    left_b = jnp.concatenate([hb[k] for k in range(Y)], axis=1)
    pk = copies.ids(6)
    for s in (2, 1, 3):
        yy, xx = lax.rem(y + s, Y), lax.rem(x + s, X)
        pa[s - 1] = mm(left_a, wa[yy].reshape(X * W, W)).astype(BF16)
        copies.start(pk + s - 1, pa.at[s - 1], ra.at[s - 1], {"tp_0": yy})
        pb[s - 1] = mm(left_b, wb[xx].reshape(Y * W, W)).astype(BF16)
        copies.start(pk + 2 + s, pb.at[s - 1], rb.at[s - 1], {"tp_1": xx})
    acc[:, 0:W] = mm(left_a, wa[y].reshape(X * W, W)) + mm(left_b, wb[x].reshape(Y * W, W))

    both(mix, "relay", -1)
    both(mix, "relay", 1)
    both(mix, "relay", 2)

    for s in range(1, 4):
        copies.landed(pk + s - 1, ra.at[s - 1], {"tp_0": lax.rem(y + s, Y)})
        copies.landed(pk + 2 + s, rb.at[s - 1], {"tp_1": lax.rem(x + s, X)})
    summed = acc[:, 0:W]
    for s in range(3):
        summed = summed + ra[s].astype(F32) + rb[s].astype(F32)
    eo[...] = summed.astype(BF16)
    ret[mine_at, :] = eo[mine_at, :]

    def give_back(i, _):
        j, dev = ring_dev(far_first(i))
        pltpu.make_async_remote_copy(
            src_ref=eo.at[pl.ds(pl.multiple_of(j * CAP, CAP), CAP)],
            dst_ref=ret.at[mine_at],
            send_sem=zsem.at[2],
            recv_sem=zsem.at[3],
            device_id=dev,
            device_id_type=MESH,
        ).start()
        return _

    lax.fori_loop(0, E - 1, give_back, 0)

    for j in (0, -1, 1, 2):
        both(mix, "far", j)
    local[4].wait()
    heads = jnp.concatenate([ho[k] for k in range(T)], axis=1)
    mix_ref[...] = mm(heads, wo[...]).astype(BF16)

    z_all(ret, 3, "recv")
    moe_out = jnp.zeros((ROWS, W), F32)
    for k in range(2):
        moe_out = moe_out + mm(oh[k], ret[...], 0, 0) * rw_ref[:, k : k + 1]
    moe_ref[...] = moe_out.astype(BF16)

    copies.drain()
    z_all(snd, 0, "send")
    z_all(eo, 2, "send")

    @pl.when(owner)
    def _():
        state_all(sts, Z - 1, 4, "send")
        state_all(sto, E - 1, 6, "send")

    @pl.when(jnp.logical_not(owner))
    def _():
        state_all(sts, Z, 4, "send")


def tables():
    half = W // 2
    inverse = 10000.0 ** (-np.arange(half, dtype=np.float64) / half)
    near = np.arange(ROWS, dtype=np.float64)[:, None] * inverse[None, :]
    base = (np.arange(E, dtype=np.float64) * ROWS)[:, None] * inverse[None, :]
    both_halves = lambda a: np.concatenate([a, a], axis=1).astype(np.float32)
    return (
        both_halves(np.cos(near)),
        both_halves(np.sin(near)),
        both_halves(np.cos(base))[:, None, :],
        both_halves(np.sin(base))[:, None, :],
    )


def on_device(
    queries, keys, values, gates, log_decay, out_weight,
    moe_rows, moe_gain, routes, route_weights, gate_proj, up_proj, down_proj,
):
    vmem = pl.BlockSpec(memory_space=pltpu.VMEM)
    hbm = pl.BlockSpec(memory_space=pl.ANY)
    scratch = [
        pltpu.VMEM((D, 256), BF16),
        pltpu.VMEM((D, 256), BF16),
        pltpu.VMEM((D, W), BF16),
        pltpu.VMEM((Y, X, W, W), BF16),
        pltpu.VMEM((X, Y, W, W), BF16),
        pltpu.VMEM((2, SLOTS, ROWS), BF16),
        pltpu.VMEM((SLOTS, W), BF16),
        pltpu.VMEM((T, SLOTS, W), BF16),
        pltpu.VMEM((SLOTS, 512), F32),
        pltpu.VMEM((X, SLOTS, W), BF16),
        pltpu.VMEM((Y, SLOTS, W), BF16),
        pltpu.VMEM((3, SLOTS, W), BF16),
        pltpu.VMEM((3, SLOTS, W), BF16),
        pltpu.VMEM((3, SLOTS, W), BF16),
        pltpu.VMEM((3, SLOTS, W), BF16),
        pltpu.VMEM((SLOTS, W), BF16),
        pltpu.VMEM((SLOTS, W), BF16),
        pltpu.VMEM((Z, 9, W), F32),
        pltpu.VMEM((E, 9, W), F32),
        pltpu.VMEM((E, 8, W), F32),
        pltpu.VMEM((Z, 8, W), F32),
        pltpu.VMEM((ROWS, W), F32),
        pltpu.VMEM((ROWS, W), BF16),
        pltpu.VMEM((ROWS, W), F32),
        pltpu.VMEM((2, W, W), F32),
        pltpu.VMEM((T, ROWS, W), BF16),
        pltpu.SemaphoreType.DMA((5,)),
        pltpu.SemaphoreType.DMA((100,)),
        pltpu.SemaphoreType.DMA((100,)),
        pltpu.SemaphoreType.DMA((8,)),
    ]
    out = jax.ShapeDtypeStruct((ROWS, W), BF16)
    return pl.pallas_call(
        kernel,
        out_shape=(out, out),
        in_specs=[vmem] * 5 + [hbm] + [vmem] * 4 + [hbm] * 3 + [vmem] * 4,
        out_specs=(vmem, vmem),
        scratch_shapes=scratch,
        compiler_params=pltpu.CompilerParams(
            collective_id=0, has_side_effects=True, vmem_limit_bytes=48 * 2**20
        ),
    )(
        queries, keys, values, gates, log_decay.reshape(2, BLOCK), out_weight,
        moe_rows, moe_gain.reshape(1, D), routes.T, route_weights,
        gate_proj.reshape(D, 256), up_proj.reshape(D, 256),
        down_proj.reshape(Y, X, 2, W, W), *tables(),
    )


def solution(mesh):
    torus = Mesh(mesh.devices.reshape(Z, C, Y, X), ("ep_0", "ep_1", "tp_0", "tp_1"))
    return jax.shard_map(
        on_device,
        mesh=torus,
        in_specs=(
            P(EP, TP), P(EP, TP), P(EP, TP), P(EP, TP), P(EP, TP), P(None, TP),
            P(EP, None), P(), P(EP, None), P(EP, None),
            P(EP, None, TP), P(EP, None, TP), P(EP, None, TP),
        ),
        out_specs=(P(EP, TP), P(EP, TP)),
        check_vma=False,
    )
```

time: 251 us -> 89.1 us (0.35)
  waiting for transfers between devices: 126 us -> 0 us
  Pallas kernels: 0 us -> 74 us
  starting transfers between devices: 38 us -> 0 us
  other arithmetic: 24.8 us -> 0 us
  between operations: 18 us -> 0.72 us
  blocking collectives: 13.4 us -> 0 us
  matrix products: 9.84 us -> 0 us
  local copies, waits for them, and re-layouts: 18.7 us -> 13.8 us
    all_gather x3 -> x0, waiting for transfers between devices: 96.3 us -> none  [the longest x1 56 us: expert_half(): lax.all_gather(hidden, TP, axis=2, tiled=True)]
    pallas_call x0 -> x1, Pallas kernels: none -> 74 us  [on_device(): pl.pallas_call(kernel, out_shape=(out, out), in_specs=[vmem] * 5 + [hbm]...]
    all_to_all x3 -> x0, starting transfers between devices: 37.9 us -> none  [the longest x1 16.7 us: expert_half(): lax.all_to_all(own_share, EP, split_axis=0, concat_axis=0, tiled=True)]
    all_to_all x3 -> x0, waiting for transfers between devices: 29.9 us -> none  [the longest x1 20.5 us: copy_for_each(): lax.all_to_all(jnp.broadcast_to(array[None], (peers, *array.shape)), axis...]
    all_gather x2 -> x0, blocking collectives: 13.4 us -> none  [the longest x1 9.98 us: whole_of(): array = lax.all_gather(array, axis, axis=dim, tiled=True)]
    mul x2 -> x0, other arithmetic: 12.2 us -> none  [the longest x1 11.5 us: retention_half(): entering = before + jnp.exp(leading)[:, :, None, None] * incoming[1][None]]
    unnamed x33, local copies, waits for them, and re-layouts: 2.57 us -> 13 us
    dot_general x7 -> x0, matrix products: 9.84 us -> none  [the longest x1 3.43 us: expert_half(): jnp.einsum('scf,fd->scd', lax.all_gather(hidden, TP, axis=2, tiled=True),...]
  transfers between devices with their start and end apart: 6 -> 0, of which waited for: 5 -> 0; matrix products, arithmetic and copies ran while one was open for 13% -> 0% of each run, Pallas kernels for 0% -> 0%
where the time goes in v1:
time: 89.1 us; the launch traced here: 88.5 us
  Pallas kernels  74 us (83%)
  local copies, waits for them, and re-layouts  13.8 us (15%)
    pallas_call x1, Pallas kernels, on_device(): pl.pallas_call(kernel, out_shape=(out, out), in_specs=[vmem] * 5 + [hbm]...  74 us
    unnamed x33, local copies, waits for them, and re-layouts  13 us

profile of v1, /device:TPU:1, one launch (start us, length us, event | category | flops | bytes accessed | tf_op | source)
XLA Modules:
  0.0 88.5 jit_solution(8426171846770513797)
XLA Ops:
  0.6 0.0 copy-start.5
  0.6 0.7 reshape.20.gain_ref
  1.4 0.0 copy-start.11
  1.4 0.0 copy-start.13
  1.4 0.0 copy-start.14
  1.4 0.8 copy.19.rw_ref
  2.2 0.0 copy-done.5
  2.2 0.0 copy-done.11
  2.3 0.0 copy-done.13
  2.3 0.0 copy-done.14
  2.3 0.0 copy-start
  2.3 1.2 %copy-done = bf16[256,2048]{1,0:T(8,128)(2,1)S(1)} copy-done((bf16[256,2048]{1,0:T(8,128)(2,1)S(1)}, bf16[256,2048]{1,0:T(8,128)(2,1)}, u32[]{:S(2)}) %copy-start) | copy-done | bytes 1048600
  3.5 0.0 copy-start.1
  3.5 1.2 %copy-done.1 = bf16[1,2048,256]{2,1,0:T(8,128)(2,1)S(1)} copy-done((bf16[1,2048,256]{2,1,0:T(8,128)(2,1)S(1)}, bf16[1,2048,256]{2,1,0:T(8,128)(2,1)}, u32[]{:S(2)}) %copy-start.1) | copy-done | bytes 1048600
  4.7 0.0 copy-start.2
  4.7 1.2 %copy-done.2 = bf16[1,2048,256]{2,1,0:T(8,128)(2,1)S(1)} copy-done((bf16[1,2048,256]{2,1,0:T(8,128)(2,1)S(1)}, bf16[1,2048,256]{2,1,0:T(8,128)(2,1)}, u32[]{:S(2)}) %copy-start.2) | copy-done | bytes 1048600
  6.0 0.0 copy-start.3
  6.0 1.2 %copy-done.3 = bf16[1,4096,128]{2,1,0:T(8,128)(2,1)S(1)} copy-done((bf16[1,4096,128]{2,1,0:T(8,128)(2,1)S(1)}, bf16[1,4096,128]{2,1,0:T(8,128)(2,1)}, u32[]{:S(2)}) %copy-start.3) | copy-done | bytes 1048600
  7.2 0.0 copy-start.4
  7.2 1.0 %copy-done.4 = bf16[2048,128]{1,0:T(8,128)(2,1)S(1)} copy-done((bf16[2048,128]{1,0:T(8,128)(2,1)S(1)}, bf16[2048,128]{1,0:T(8,128)(2,1)}, u32[]{:S(2)}) %copy-start.4) | copy-done | bytes 524312
  8.2 0.0 copy-start.6
  8.2 0.9 %copy-done.6 = f32[256,128]{1,0:T(8,128)S(1)} copy-done((f32[256,128]{1,0:T(8,128)S(1)}, f32[256,128]{1,0:T(8,128)}, u32[]{:S(2)}) %copy-start.6) | copy-done | bytes 131096
  9.1 0.0 copy-start.7
  9.1 0.8 copy-done.7
  10.0 0.0 copy-start.8
  10.0 0.8 copy-done.8
  10.8 0.0 copy-start.9
  10.8 0.8 copy-done.9
  11.6 0.0 copy-start.10
  11.6 0.8 copy-done.10
  12.5 0.0 copy-start.12
  12.5 0.7 copy-done.12
  13.2 74.0 %shard_map.176 = (bf16[256,128]{1,0:T(8,128)(2,1)S(1)}, bf16[256,128]{1,0:T(8,128)(2,1)S(1)}) custom-call(bf16[256,128]{1,0:T(8,128)(2,1)S(1)} %copy-done.7, bf16[256,128]{1,0:T(8,128)(2,1)S(1)} %copy-done.8, bf16[256,128]{1,0:T(8,128)(2,1)S(1)} %copy-done.9, bf16[256,128]{1,0:T(8,128)(2,1)S(1)} %copy-done.10, f32[2,128]{1,0:T(2,128)S(1)} %bitcast.9, ...), custom_call_target="tpu_custom_call" | custom-call | tf_op jit(solution)/shard_map/pallas_call | solution.py:602
  87.3 0.6 copy.22
  87.9 0.6 copy.23
Async XLA Ops:
  0.6 1.6 %copy-start.5 = (f32[256,128]{1,0:T(8,128)S(1)}, f32[256,128]{1,0:T(8,128)}, u32[]{:S(2)}) copy-start(f32[256,128]{1,0:T(8,128)} %constant.9.clone.sr_ref) | copy-start | bytes 393220
  1.4 0.9 copy-start.11
  1.4 0.9 copy-start.13
  1.4 0.9 %copy-start.14 = (f32[256,1]{0,1:T(1,128)S(1)}, f32[256,1]{0,1:T(1,128)}, u32[]{:S(2)}) copy-start(f32[256,1]{0,1:T(1,128)} %param.21) | copy-start | bytes 3076
  2.3 1.2 %copy-start = (bf16[256,2048]{1,0:T(8,128)(2,1)S(1)}, bf16[256,2048]{1,0:T(8,128)(2,1)}, u32[]{:S(2)}) copy-start(bf16[256,2048]{1,0:T(8,128)(2,1)} %rows_ref.1) | copy-start | bytes 3145732
  3.5 1.2 %copy-start.1 = (bf16[1,2048,256]{2,1,0:T(8,128)(2,1)S(1)}, bf16[1,2048,256]{2,1,0:T(8,128)(2,1)}, u32[]{:S(2)}) copy-start(bf16[1,2048,256]{2,1,0:T(8,128)(2,1)} %param.27) | copy-start | bytes 3145732
  4.7 1.2 %copy-start.2 = (bf16[1,2048,256]{2,1,0:T(8,128)(2,1)S(1)}, bf16[1,2048,256]{2,1,0:T(8,128)(2,1)}, u32[]{:S(2)}) copy-start(bf16[1,2048,256]{2,1,0:T(8,128)(2,1)} %param.28) | copy-start | bytes 3145732
  6.0 1.2 %copy-start.3 = (bf16[1,4096,128]{2,1,0:T(8,128)(2,1)S(1)}, bf16[1,4096,128]{2,1,0:T(8,128)(2,1)}, u32[]{:S(2)}) copy-start(bf16[1,4096,128]{2,1,0:T(8,128)(2,1)} %param.29) | copy-start | bytes 3145732
  7.2 1.0 %copy-start.4 = (bf16[2048,128]{1,0:T(8,128)(2,1)S(1)}, bf16[2048,128]{1,0:T(8,128)(2,1)}, u32[]{:S(2)}) copy-start(bf16[2048,128]{1,0:T(8,128)(2,1)} %wo_hbm.1) | copy-start | bytes 1572868
  8.2 0.9 %copy-start.6 = (f32[256,128]{1,0:T(8,128)S(1)}, f32[256,128]{1,0:T(8,128)}, u32[]{:S(2)}) copy-start(f32[256,128]{1,0:T(8,128)} %constant.8.clone.cr_ref) | copy-start | bytes 393220
  9.1 0.8 copy-start.7
  10.0 0.8 copy-start.8
  10.8 0.8 copy-start.9
  11.6 0.8 copy-start.10
  12.5 0.7 copy-start.12

commit v2 on v1

--- a/solution.py
+++ b/solution.py
@@ -19,6 +19,7 @@
 D = 2048
 W = 128
 BLOCK = 128
+NEAR = 8
 EP = ("ep_0", "ep_1")
 TP = ("tp_0", "tp_1")
 
@@ -77,13 +78,13 @@
 
 
 class Spread:
-    def __init__(self, copies, buf, h0, n, first):
-        self.c, self.buf, self.h0, self.n, self.first = copies, buf, h0, n, first
+    def __init__(self, copies, buf, h0, n, axis):
+        self.c, self.buf, self.h0, self.n, self.axis = copies, buf, h0, n, axis
         self.k = copies.ids(20)
 
     def offset(self, dp, dq):
         y, x = self.c.place
-        dy, dx = (dq, dp) if self.first == "x" else (dp, dq)
+        dy, dx = (dq, dp) if self.axis == "x" else (dp, dq)
         return lax.rem(y + dy + Y, Y), lax.rem(x + dx + X, X)
 
     def ref(self, dp, dq, part=None):
@@ -108,38 +109,39 @@
     def turn(self, j):
         return {0: 0, -1: 1, 1: 2, 2: 3}[j]
 
-    def first_own(self):
-        self.go(0, (0, 0), (1, 0))
-        self.go(1, (0, 0), (-1, 0))
+    def own(self):
+        for k, to in enumerate(((1, 0), (-1, 0), (2, 0))):
+            self.go(k, (0, 0), to)
+        self.go(4, (0, 0), (0, 1))
+        self.go(5, (0, 0), (0, -1))
 
     def across(self, j):
         base = 4 + 4 * self.turn(j)
-        self.go(base, (j, 0), (0, 1))
-        self.go(base + 1, (j, 0), (0, -1))
-
-    def first_left(self):
-        self.got(0, (-1, 0))
-        self.go(2, (-1, 0), (1, 0), 0)
-
-    def first_right(self):
-        self.got(1, (1, 0))
-        self.go(3, (1, 0), (-1, 0), 1)
-
-    def first_far(self):
-        self.got(2, (2, 0), 0)
-        self.got(3, (2, 0), 1)
-
-    def relay(self, j):
-        base = 4 + 4 * self.turn(j)
-        self.got(base, (j, -1))
-        self.go(base + 2, (j, -1), (0, 1), 0)
-        self.got(base + 1, (j, 1))
-        self.go(base + 3, (j, 1), (0, -1), 1)
-
-    def far(self, j):
-        base = 4 + 4 * self.turn(j)
-        self.got(base + 2, (j, 2), 0)
-        self.got(base + 3, (j, 2), 1)
+        for k, to in enumerate((1, -1, 2)):
+            self.go(base + k, (j, 0), (0, to))
+
+    def first(self):
+        for k, j in enumerate((-1, 1, 2)):
+            self.got(k, (j, 0))
+            self.across(j)
+
+    def relay(self):
+        self.got(4, (0, -1))
+        self.go(6, (0, -1), (0, 1), 0)
+        self.got(5, (0, 1))
+        self.go(7, (0, 1), (0, -1), 1)
+
+    def near(self):
+        for j in (-1, 1, 2):
+            base = 4 + 4 * self.turn(j)
+            self.got(base, (j, -1))
+            self.got(base + 1, (j, 1))
+
+    def far(self):
+        self.got(6, (0, 2), 0)
+        self.got(7, (0, 2), 1)
+        for j in (-1, 1, 2):
+            self.got(4 + 4 * self.turn(j) + 2, (j, 2))
 
 
 def both(pair, step, *args):
@@ -148,11 +150,13 @@
 
 
 def kernel(
-    q_ref, k_ref, v_ref, g_ref, ld_ref, wo_hbm, rows_ref, gain_ref, routes_ref, rw_ref,
-    wg_hbm, wu_hbm, wd_hbm, cr_ref, sr_ref, cb_ref, sb_ref,
-    mix_ref, moe_ref,
+    q_hbm, k_hbm, v_hbm, g_hbm, ld_hbm, wo_hbm, rows_hbm, gain_hbm, routes_hbm, rw_hbm,
+    wg_hbm, wu_hbm, wd_hbm, cr_hbm, sr_hbm, cb_hbm, sb_hbm,
+    mix_hbm, moe_hbm,
+    q_ref, k_ref, v_ref, g_ref, ld_ref, rows_ref, gain_ref, routes_ref, rw_ref,
+    cr_ref, sr_ref, cb_ref, sb_ref, mix_ref, moe_ref,
     wg, wu, wo, wa, wb, oh, snd, rbuf, acc, ha, hb, pa, pb, ra, rb, eo, ret,
-    sts, str_, sto, sti, ins, rotq, cum, upd, ho,
+    sts, str_, sto, sti, ins, rotq, cum, upd, ho, psum,
     lsem, send, recv, zsem,
 ):
     z, c = lax.axis_index("ep_0"), lax.axis_index("ep_1")
@@ -162,6 +166,27 @@
     copies = Copies(send, recv, (y, x))
 
     barrier = pltpu.get_barrier_semaphore()
+    wd_rows = wd_hbm
+    routed = (
+        (routes_hbm, routes_ref), (rows_hbm, rows_ref), (gain_hbm, gain_ref), (rw_hbm, rw_ref),
+    )
+    mixed = (
+        (k_hbm, k_ref), (q_hbm, q_ref), (v_hbm, v_ref), (ld_hbm, ld_ref), (cr_hbm, cr_ref),
+        (sr_hbm, sr_ref), (cb_hbm.at[e], cb_ref), (sb_hbm.at[e], sb_ref), (g_hbm, g_ref),
+    )
+    held = (
+        (wg_hbm, wg), (wu_hbm, wu), (wd_rows.at[y, :, 0], wa.at[y]),
+        (wd_rows.at[:, x, 1], wb.at[x]), (wo_hbm, wo),
+    )
+    local = [
+        pltpu.make_async_copy(src, dst, lsem.at[n])
+        for n, (src, dst) in enumerate(routed + mixed + held)
+    ]
+    for copy in local:
+        copy.start()
+    routed = local[: len(routed)]
+    mixed = local[len(routed) : -len(held)]
+    local = local[-len(held) :]
 
     def ring_dev(d):
         j = lax.rem(e + d, E)
@@ -180,16 +205,8 @@
             barrier, inc=1, device_id={"tp_1": lax.rem(x + s, X)}, device_id_type=MESH
         )
 
-    wd_rows = wd_hbm
-    local = [
-        pltpu.make_async_copy(wg_hbm, wg, lsem.at[0]),
-        pltpu.make_async_copy(wu_hbm, wu, lsem.at[1]),
-        pltpu.make_async_copy(wd_rows.at[y, :, 0], wa.at[y], lsem.at[2]),
-        pltpu.make_async_copy(wd_rows.at[:, x, 1], wb.at[x], lsem.at[3]),
-        pltpu.make_async_copy(wo_hbm, wo, lsem.at[4]),
-    ]
-    for copy in local:
-        copy.start()
+    for copy in routed:
+        copy.wait()
 
     slot_id = lax.broadcasted_iota(jnp.int32, (SLOTS, ROWS), 0)
     expert_of = slot_id // CAP
@@ -206,13 +223,15 @@
         oh[k] = jnp.logical_and(named[k], here).astype(F32).astype(BF16)
 
     lanes = pl.ds(pl.multiple_of(t * W, W), W)
+    gain_at = lax.broadcasted_iota(jnp.int32, (T, W), 0) == t
+    gain = jnp.sum(jnp.where(gain_at, gain_ref[...].astype(F32), 0.0), axis=0, keepdims=True)
 
     def squares(r, _):
         rows = pl.ds(pl.multiple_of(r * 64, 64), 64)
         full = rows_ref[rows, :].astype(F32)
         mean = jnp.sum(full * full, axis=-1, keepdims=True) * (1.0 / D)
         mine = rows_ref[rows, lanes].astype(F32)
-        normed = mine * lax.rsqrt(mean + 1e-06) * gain_ref[:, lanes].astype(F32)
+        normed = mine * lax.rsqrt(mean + 1e-06) * gain
         rotq[rows, :] = normed.astype(BF16)
         return _
 
@@ -221,27 +240,43 @@
     picked = mm(oh[0] + oh[1], normed)
     snd[...] = picked.astype(BF16)
     mine_at = pl.ds(pl.multiple_of(e * CAP, CAP), CAP)
-    rbuf[t, mine_at, :] = snd[mine_at, :]
+    own_rows = slice(NEAR * CAP, (NEAR + 1) * CAP)
+    rbuf[t, own_rows, :] = snd[mine_at, :]
 
     pl.semaphore_wait(barrier, E - 1 + 6)
 
-    def far_first(i):
+    def near_d(i):
+        even = 1 - lax.rem(i, 2)
+        return even * (i // 2 - NEAR) + (1 - even) * (NEAR - 1 - i // 2)
+
+    def far_d(i):
         half = (i + 1) // 2
         return E // 2 + half * (1 - 2 * lax.rem(i, 2))
 
-    def dispatch(i, _):
-        j, dev = ring_dev(far_first(i))
+    def tile(k):
+        return pl.ds(pl.multiple_of(k * CAP, CAP), CAP)
+
+    def dispatch(d, sem):
+        j, dev = ring_dev(E - d)
         pltpu.make_async_remote_copy(
-            src_ref=snd.at[pl.ds(pl.multiple_of(j * CAP, CAP), CAP)],
-            dst_ref=rbuf.at[t, mine_at],
+            src_ref=snd.at[tile(j)],
+            dst_ref=rbuf.at[t, tile(NEAR + d)],
             send_sem=zsem.at[0],
-            recv_sem=zsem.at[1],
+            recv_sem=zsem.at[sem],
             device_id=dev,
             device_id_type=MESH,
         ).start()
-        return _
-
-    lax.fori_loop(0, E - 1, dispatch, 0)
+
+    def dispatch_near(i, carry):
+        dispatch(near_d(i), 1)
+        return carry
+
+    def dispatch_far(i, carry):
+        dispatch(far_d(i), 8)
+        return carry
+
+    lax.fori_loop(0, E // 2 - 1, dispatch_near, 0)
+    lax.fori_loop(0, E // 2, dispatch_far, 0)
 
     wk = copies.ids(6)
     for s in (2, 1, 3):
@@ -249,7 +284,9 @@
         copies.start(wk + s - 1, wd_rows.at[yy, :, 0], wa.at[y], {"tp_0": yy})
         copies.start(wk + 2 + s, wd_rows.at[:, xx, 1], wb.at[x], {"tp_1": xx})
 
-    cb, sb = cb_ref[e], sb_ref[e]
+    for copy in mixed:
+        copy.wait()
+    cb, sb = cb_ref[...], sb_ref[...]
     cos = cb * cr_ref[...] - sb * sr_ref[...]
 
     def signed(first, second):
@@ -320,8 +357,8 @@
 
     lax.fori_loop(0, Z, give, 0)
 
-    def z_all(buf, sem, kind):
-        part = buf.at[pl.ds(0, (E - 1) * CAP)]
+    def tiles(buf, count, sem, kind):
+        part = buf.at[pl.ds(0, count * CAP)]
         copy = pltpu.make_async_remote_copy(
             src_ref=part, dst_ref=part, send_sem=zsem.at[sem], recv_sem=zsem.at[sem],
             device_id={"tp_1": lax.rem(x + 1, X)}, device_id_type=MESH,
@@ -331,11 +368,146 @@
         else:
             copy.wait_send()
 
-    z_all(rbuf.at[t], 1, "recv")
-    moe = (Spread(copies, rbuf, 0, ROWS, "x"), Spread(copies, rbuf, ROWS, ROWS, "y"))
-    both(moe, "first_own")
-    both(moe, "across", 0)
-
+    HALF = ROWS // 2
+    moe = [
+        (
+            Spread(copies, rbuf, ROWS * n, HALF, "x"),
+            Spread(copies, rbuf, ROWS * n + HALF, HALF, "y"),
+        )
+        for n in range(2)
+    ]
+    hop_ids = [copies.ids(8) for _ in range(2)]
+    sum_ids = [copies.ids(6) for _ in range(2)]
+
+    def chunk(n):
+        return slice(n * ROWS, (n + 1) * ROWS)
+
+    def spread_own(n):
+        tiles(rbuf.at[t], E // 2 - 1 + n, 1 if n == 0 else 8, "recv")
+        both(moe[n], "own")
+
+    def spread_first(n):
+        both(moe[n], "first")
+        both(moe[n], "relay")
+
+    def gather_group(half, dqs, fresh):
+        rows = pl.ds(half.h0, half.n)
+        blocks = []
+        for dq in dqs:
+            for k in range(4):
+                yy, xx = half.offset(k, dq)
+                blocks.append(yy * X + xx)
+        left = jnp.concatenate([rbuf[b, rows, :] for b in blocks], axis=1)
+        for at, weight in ((0, wg), (256, wu)):
+            right = jnp.concatenate(
+                [weight[pl.ds(pl.multiple_of(b * W, W), W), :] for b in blocks], axis=0
+            )
+            product = mm(left, right)
+            if fresh:
+                acc[rows, at : at + 256] = product
+            else:
+                acc[rows, at : at + 256] += product
+
+    def gather(n, *dqs):
+        for half in moe[n]:
+            gather_group(half, dqs, dqs == (0,))
+
+    def hop(n, side, block, to):
+        axis, buf, me = (("tp_1", ha, x), ("tp_0", hb, y))[side]
+        ref = buf.at[lax.rem(me + block, 4), pl.ds(n * ROWS, ROWS)]
+        return hop_ids[n] + 4 * side + to, ref, {axis: lax.rem(me + to, 4)}
+
+    def hidden_own(n):
+        both(moe[n], "near")
+        gather(n, 1, -1)
+        both(moe[n], "far")
+        gather(n, 2)
+        rows = chunk(n)
+        hidden = (silu(acc[rows, 0:256]) * acc[rows, 256:512]).astype(BF16)
+        ha[x, rows, :] = hidden[:, 0:W]
+        hb[y, rows, :] = hidden[:, W : 2 * W]
+        for to in (2, 1, 3):
+            for side in range(2):
+                kk, ref, dev = hop(n, side, 0, to)
+                copies.start(kk, ref, ref, dev)
+
+    def partial(n, side, offsets):
+        buf, weight, me, other = ((ha, wa, x, y), (hb, wb, y, x))[side]
+        rows = chunk(n)
+        held = [lax.rem(me + o, 4) for o in offsets]
+        left = jnp.concatenate([buf[b, rows, :] for b in held], axis=1)
+        right = jnp.concatenate(
+            [
+                jnp.concatenate([weight[lax.rem(other + s, 4), b] for b in held], axis=0)
+                for s in range(4)
+            ],
+            axis=1,
+        )
+        return mm(left, right)
+
+    def down_own(n):
+        for side in range(2):
+            psum[side, chunk(n), :] = partial(n, side, (0,))
+
+    def down_rest(n):
+        for side in range(2):
+            for to in range(1, 4):
+                kk, ref, dev = hop(n, side, 4 - to, to)
+                copies.landed(kk, ref, dev)
+        rows = chunk(n)
+        at = pl.ds(n * ROWS, ROWS)
+        for side in range(2):
+            out, into, axis, me = ((pa, ra, "tp_0", y), (pb, rb, "tp_1", x))[side]
+            whole = psum[side, rows, :] + partial(n, side, (1, 3, 2))
+            for s in (2, 1, 3):
+                out[s - 1, rows, :] = whole[:, s * W : (s + 1) * W].astype(BF16)
+                copies.start(
+                    sum_ids[n] + 3 * side + s - 1, out.at[s - 1, at], into.at[s - 1, at],
+                    {axis: lax.rem(me + s, 4)},
+                )
+            psum[side, rows, 0:W] = whole[:, 0:W]
+
+    def give_back(d):
+        j, dev = ring_dev(E + d)
+        pltpu.make_async_remote_copy(
+            src_ref=eo.at[tile(NEAR + d)],
+            dst_ref=ret.at[mine_at],
+            send_sem=zsem.at[2],
+            recv_sem=zsem.at[3],
+            device_id=dev,
+            device_id_type=MESH,
+        ).start()
+
+    def back_near(i, carry):
+        give_back(near_d(i))
+        return carry
+
+    def back_far(i, carry):
+        give_back(far_d(i))
+        return carry
+
+    def finish(n):
+        rows = chunk(n)
+        at = pl.ds(n * ROWS, ROWS)
+        summed = psum[0, rows, 0:W] + psum[1, rows, 0:W]
+        for side in range(2):
+            into, axis, me = ((ra, "tp_0", y), (rb, "tp_1", x))[side]
+            for s in range(1, 4):
+                copies.landed(
+                    sum_ids[n] + 3 * side + s - 1, into.at[s - 1, at], {axis: lax.rem(me + s, 4)}
+                )
+                summed = summed + into[s - 1, rows, :].astype(F32)
+        eo[rows, :] = summed.astype(BF16)
+        if n == 0:
+            ret[mine_at, :] = eo[own_rows, :]
+            lax.fori_loop(0, E // 2 - 1, back_near, 0)
+        else:
+            lax.fori_loop(0, E // 2, back_far, 0)
+
+    spread_own(0)
+
+    spread_first(0)
+    spread_own(1)
     def state_all(buf, count, sem, kind):
         part = buf.at[pl.ds(0, count)]
         copy = pltpu.make_async_remote_copy(
@@ -358,7 +530,7 @@
         sti[z] = sto[e]
 
         def back(i, _):
-            j, dev = ring_dev(far_first(i))
+            j, dev = ring_dev(far_d(i))
             pltpu.make_async_remote_copy(
                 src_ref=sto.at[j],
                 dst_ref=sti.at[z],
@@ -371,36 +543,20 @@
 
         lax.fori_loop(0, E - 1, back, 0)
 
-    both(moe, "first_left")
-    both(moe, "across", -1)
-    both(moe, "first_right")
-    both(moe, "across", 1)
-    both(moe, "relay", 0)
-    both(moe, "first_far")
-    both(moe, "across", 2)
-
     local[0].wait()
     local[1].wait()
-
-    def gather_group(half, dq, fresh):
-        rows = pl.ds(half.h0, half.n)
-        blocks, left = [], []
-        for k in range(4):
-            yy, xx = half.offset(k, dq)
-            blocks.append(yy * X + xx)
-        left = jnp.concatenate([rbuf[b, rows, :] for b in blocks], axis=1)
-        for at, weight in ((0, wg), (256, wu)):
-            right = jnp.concatenate(
-                [weight[pl.ds(pl.multiple_of(b * W, W), W), :] for b in blocks], axis=0
-            )
-            product = mm(left, right)
-            if fresh:
-                acc[rows, at : at + 256] = product
-            else:
-                acc[rows, at : at + 256] += product
-
-    for half in moe:
-        gather_group(half, 0, True)
+    gather(0, 0)
+    spread_first(1)
+    hidden_own(0)
+    local[2].wait()
+    local[3].wait()
+    for s in range(1, 4):
+        copies.landed(wk + s - 1, wa.at[lax.rem(y + Y - s, Y)], {"tp_0": lax.rem(y + s, Y)})
+        copies.landed(wk + 2 + s, wb.at[lax.rem(x + X - s, X)], {"tp_1": lax.rem(x + s, X)})
+    down_own(0)
+    gather(1, 0)
+    down_rest(0)
+    hidden_own(1)
 
     @pl.when(owner)
     def _():
@@ -422,119 +578,34 @@
         ho[t, rows, :] = (retained * lax.rsqrt(mean + 1e-05) * silu(gate)).astype(BF16)
         entering = upd[1] * entering + upd[0]
     mix = (Spread(copies, ho, 0, BLOCK, "x"), Spread(copies, ho, BLOCK, BLOCK, "y"))
-    both(mix, "first_own")
-    both(mix, "across", 0)
-
-    both(moe, "relay", -1)
-    both(moe, "relay", 1)
-    both(moe, "relay", 2)
-    for half in moe:
-        gather_group(half, -1, False)
-        gather_group(half, 1, False)
-    for j in (0, -1, 1, 2):
-        both(moe, "far", j)
-    for half in moe:
-        gather_group(half, 2, False)
-
-    hidden = (silu(acc[:, 0:256]) * acc[:, 256:512]).astype(BF16)
-    ha[x] = hidden[:, 0:W]
-    hb[y] = hidden[:, W : 2 * W]
-
-    hk = copies.ids(8)
-
-    def hop(k, axis, buf, block, to, part=None):
-        me, size = (x, X) if axis == "tp_1" else (y, Y)
-        ref = buf.at[lax.rem(me + block + size, size)]
-        if part is not None:
-            ref = ref.at[pl.ds(part * ROWS, ROWS)]
-        return k, ref, {axis: lax.rem(me + to + size, size)}
-
-    hsides = (("tp_1", ha, hk), ("tp_0", hb, hk + 4))
-    for axis, buf, k in hsides:
-        for n, to in ((0, 1), (1, -1)):
-            kk, ref, dev = hop(k + n, axis, buf, 0, to)
-            copies.start(kk, ref, ref, dev)
-
-    both(mix, "first_left")
-    both(mix, "across", -1)
-    both(mix, "first_right")
-    both(mix, "across", 1)
-
-    for n, frm, part in ((0, -1, 0), (1, 1, 1)):
-        for axis, buf, k in hsides:
-            kk, ref, dev = hop(k + n, axis, buf, frm, 1)
-            copies.landed(kk, ref, dev)
-            kk, ref, dev = hop(k + 2 + n, axis, buf, frm, -frm, part)
-            copies.start(kk, ref, ref, dev)
-
-    both(mix, "relay", 0)
-    both(mix, "first_far")
-    both(mix, "across", 2)
-
-    for axis, buf, k in hsides:
-        for n in range(2):
-            kk, ref, dev = hop(k + 2 + n, axis, buf, 2, 1, n)
-            copies.landed(kk, ref, dev)
-
-    local[2].wait()
-    local[3].wait()
-    for s in range(1, 4):
-        copies.landed(wk + s - 1, wa.at[lax.rem(y + Y - s, Y)], {"tp_0": lax.rem(y + s, Y)})
-        copies.landed(wk + 2 + s, wb.at[lax.rem(x + X - s, X)], {"tp_1": lax.rem(x + s, X)})
-
-    left_a = jnp.concatenate([ha[k] for k in range(X)], axis=1)
-    left_b = jnp.concatenate([hb[k] for k in range(Y)], axis=1)
-    pk = copies.ids(6)
-    for s in (2, 1, 3):
-        yy, xx = lax.rem(y + s, Y), lax.rem(x + s, X)
-        pa[s - 1] = mm(left_a, wa[yy].reshape(X * W, W)).astype(BF16)
-        copies.start(pk + s - 1, pa.at[s - 1], ra.at[s - 1], {"tp_0": yy})
-        pb[s - 1] = mm(left_b, wb[xx].reshape(Y * W, W)).astype(BF16)
-        copies.start(pk + 2 + s, pb.at[s - 1], rb.at[s - 1], {"tp_1": xx})
-    acc[:, 0:W] = mm(left_a, wa[y].reshape(X * W, W)) + mm(left_b, wb[x].reshape(Y * W, W))
-
-    both(mix, "relay", -1)
-    both(mix, "relay", 1)
-    both(mix, "relay", 2)
-
-    for s in range(1, 4):
-        copies.landed(pk + s - 1, ra.at[s - 1], {"tp_0": lax.rem(y + s, Y)})
-        copies.landed(pk + 2 + s, rb.at[s - 1], {"tp_1": lax.rem(x + s, X)})
-    summed = acc[:, 0:W]
-    for s in range(3):
-        summed = summed + ra[s].astype(F32) + rb[s].astype(F32)
-    eo[...] = summed.astype(BF16)
-    ret[mine_at, :] = eo[mine_at, :]
-
-    def give_back(i, _):
-        j, dev = ring_dev(far_first(i))
-        pltpu.make_async_remote_copy(
-            src_ref=eo.at[pl.ds(pl.multiple_of(j * CAP, CAP), CAP)],
-            dst_ref=ret.at[mine_at],
-            send_sem=zsem.at[2],
-            recv_sem=zsem.at[3],
-            device_id=dev,
-            device_id_type=MESH,
-        ).start()
-        return _
-
-    lax.fori_loop(0, E - 1, give_back, 0)
-
-    for j in (0, -1, 1, 2):
-        both(mix, "far", j)
+
+    down_own(1)
+    finish(0)
+    down_rest(1)
+    both(mix, "own")
+    finish(1)
+    both(mix, "first")
+    both(mix, "relay")
+    both(mix, "near")
+    both(mix, "far")
     local[4].wait()
     heads = jnp.concatenate([ho[k] for k in range(T)], axis=1)
     mix_ref[...] = mm(heads, wo[...]).astype(BF16)
-
-    z_all(ret, 3, "recv")
+    mix_out = pltpu.make_async_copy(mix_ref, mix_hbm, lsem.at[0])
+    mix_out.start()
+
+    tiles(ret, E - 1, 3, "recv")
     moe_out = jnp.zeros((ROWS, W), F32)
     for k in range(2):
-        moe_out = moe_out + mm(oh[k], ret[...], 0, 0) * rw_ref[:, k : k + 1]
+        share = jnp.transpose(jnp.broadcast_to(rw_ref[k : k + 1, :], (W, ROWS)))
+        moe_out = moe_out + mm(oh[k], ret[...], 0, 0) * share
     moe_ref[...] = moe_out.astype(BF16)
+    moe_copy = pltpu.make_async_copy(moe_ref, moe_hbm, lsem.at[1])
+    moe_copy.start()
 
     copies.drain()
-    z_all(snd, 0, "send")
-    z_all(eo, 2, "send")
+    tiles(snd, E - 1, 0, "send")
+    tiles(eo, E - 1, 2, "send")
 
     @pl.when(owner)
     def _():
@@ -544,6 +615,8 @@
     @pl.when(jnp.logical_not(owner))
     def _():
         state_all(sts, Z, 4, "send")
+    mix_out.wait()
+    moe_copy.wait()
 
 
 def tables():
@@ -564,9 +637,24 @@
     queries, keys, values, gates, log_decay, out_weight,
     moe_rows, moe_gain, routes, route_weights, gate_proj, up_proj, down_proj,
 ):
+    hbm = pl.BlockSpec(memory_space=pltpu.HBM)
     vmem = pl.BlockSpec(memory_space=pltpu.VMEM)
-    hbm = pl.BlockSpec(memory_space=pl.ANY)
     scratch = [
+        pltpu.VMEM((ROWS, W), BF16),
+        pltpu.VMEM((ROWS, W), BF16),
+        pltpu.VMEM((ROWS, W), BF16),
+        pltpu.VMEM((ROWS, W), BF16),
+        pltpu.VMEM((2, BLOCK), F32),
+        pltpu.VMEM((ROWS, D), BF16),
+        pltpu.VMEM((T, W), BF16),
+        pltpu.VMEM((2, ROWS), jnp.int32),
+        pltpu.VMEM((2, ROWS), F32),
+        pltpu.VMEM((ROWS, W), F32),
+        pltpu.VMEM((ROWS, W), F32),
+        pltpu.VMEM((1, W), F32),
+        pltpu.VMEM((1, W), F32),
+        pltpu.VMEM((ROWS, W), BF16),
+        pltpu.VMEM((ROWS, W), BF16),
         pltpu.VMEM((D, 256), BF16),
         pltpu.VMEM((D, 256), BF16),
         pltpu.VMEM((D, W), BF16),
@@ -593,24 +681,25 @@
         pltpu.VMEM((ROWS, W), F32),
         pltpu.VMEM((2, W, W), F32),
         pltpu.VMEM((T, ROWS, W), BF16),
-        pltpu.SemaphoreType.DMA((5,)),
-        pltpu.SemaphoreType.DMA((100,)),
-        pltpu.SemaphoreType.DMA((100,)),
-        pltpu.SemaphoreType.DMA((8,)),
+        pltpu.VMEM((2, SLOTS, 512), F32),
+        pltpu.SemaphoreType.DMA((18,)),
+        pltpu.SemaphoreType.DMA((160,)),
+        pltpu.SemaphoreType.DMA((160,)),
+        pltpu.SemaphoreType.DMA((9,)),
     ]
     out = jax.ShapeDtypeStruct((ROWS, W), BF16)
     return pl.pallas_call(
         kernel,
         out_shape=(out, out),
-        in_specs=[vmem] * 5 + [hbm] + [vmem] * 4 + [hbm] * 3 + [vmem] * 4,
-        out_specs=(vmem, vmem),
+        in_specs=[hbm] * 17,
+        out_specs=(hbm, hbm),
         scratch_shapes=scratch,
         compiler_params=pltpu.CompilerParams(
-            collective_id=0, has_side_effects=True, vmem_limit_bytes=48 * 2**20
+            collective_id=0, has_side_effects=True, vmem_limit_bytes=67043328
         ),
     )(
         queries, keys, values, gates, log_decay.reshape(2, BLOCK), out_weight,
-        moe_rows, moe_gain.reshape(1, D), routes.T, route_weights,
+        moe_rows, moe_gain.reshape(T, W), routes.T, route_weights.T,
         gate_proj.reshape(D, 256), up_proj.reshape(D, 256),
         down_proj.reshape(Y, X, 2, W, W), *tables(),
     )

time: 89.1 us -> 73.3 us (0.82)
  the two profiles are of different devices: /device:TPU:1 before, /device:TPU:32 now
where the time goes in v2:
time: 73.3 us; the launch traced here: 73.1 us
  Pallas kernels  70.4 us (96%)
  local copies, waits for them, and re-layouts  2.14 us (3%)
    pallas_call x1, Pallas kernels, on_device(): pl.pallas_call(kernel, out_shape=(out, out), in_specs=[hbm] * 17, out_spe...  70.4 us
    unnamed x4, local copies, waits for them, and re-layouts  2.14 us

profile of v2, /device:TPU:32, one launch (start us, length us, event | category | flops | bytes accessed | tf_op | source)
XLA Modules:
  0.0 73.1 jit_solution(9165127137822684977)
XLA Ops:
  0.6 70.4 %shard_map.176 = (bf16[256,128]{1,0:T(8,128)(2,1)}, bf16[256,128]{1,0:T(8,128)(2,1)}) custom-call(bf16[256,128]{1,0:T(8,128)(2,1)} %q_hbm.1, bf16[256,128]{1,0:T(8,128)(2,1)} %k_hbm.1, bf16[256,128]{1,0:T(8,128)(2,1)} %v_hbm.1, bf16[256,128]{1,0:T(8,128)(2,1)} %g_hbm.1, f32[2,128]{1,0:T(2,128)} %bitcast.13, bf16[2048,128]{1,0:T(8,128)(2,1)} %wo_hbm.1, ...), custom_call_target="tpu_custom_call" | custom-call | tf_op jit(solution)/shard_map/pallas_call | solution.py:691
  71.0 0.0 copy-start
  71.0 1.5 %copy.21 = bf16[256,128]{1,0:T(8,128)(2,1)} copy(bf16[256,128]{1,0:T(8,128)(2,1)} %get-tuple-element.4) | data formatting | bytes 131072
  72.5 0.0 copy-done
  72.5 0.6 copy.22
Async XLA Ops:
  71.0 1.5 %copy-start = (bf16[256,128]{1,0:T(8,128)(2,1)S(1)}, bf16[256,128]{1,0:T(8,128)(2,1)}, u32[]{:S(2)}) copy-start(bf16[256,128]{1,0:T(8,128)(2,1)} %get-tuple-element.5) | copy-start | bytes 196612

commit v3 on v2

v3 whole, which is shorter than its diff:
```python
import jax
import jax.numpy as jnp
import numpy as np
from jax import lax
from jax.experimental import pallas as pl
from jax.experimental.pallas import tpu as pltpu
from jax.sharding import Mesh
from jax.sharding import PartitionSpec as P

MESH = pl.DeviceIdType.MESH
F32 = jnp.float32
BF16 = jnp.bfloat16
Z, C, Y, X = 16, 2, 4, 4
E = Z * C
T = Y * X
ROWS = 256
SLOTS = 2 * ROWS
CAP = SLOTS // E
D = 2048
W = 128
BLOCK = 128
CHUNKS = 4
ORDER = (
    "O0", "F0", "O1", "O2", "O3", "W0", "F1", "F2", "F3", "S0", "L0", "L1", "L2", "L3", "U0",
    "H0", "H1", "H2", "H3", "R0", "M0", "V0", "K1", "D1", "K2", "D2", "K0", "D0", "K3", "D3",
    "M1", "X1", "X2", "X0", "X3", "M2", "M3",
)
RELAY_ROWS = (1, 1, 1, 1)
RELAY_HIDDEN = (0, 0, 0, 0)
RELAY_HEADS = 1
CHUNK = SLOTS // CHUNKS
OWN = 4
EP = ("ep_0", "ep_1")
TP = ("tp_0", "tp_1")


def mm(a, b, ca=1, cb=0):
    return lax.dot_general(a, b, (((ca,), (cb,)), ((), ())), preferred_element_type=F32)


def parts_of(a, count):
    found = []
    for k in range(count):
        piece = a.astype(BF16)
        found.append(piece)
        if k + 1 < count:
            a = a - piece.astype(F32)
    return found


def silu(v):
    return v / (1.0 + jnp.exp(-v))


def chosen(relayed, onward, straight):
    act = (straight, onward)
    if relayed < 2:
        if act[relayed] is not None:
            act[relayed]()
        return
    for core in range(2):
        if act[core] is not None:
            pl.when(lax.axis_index("ep_1") == core)(act[core])


def rows_in(buf, rows):
    count = 1
    while rows % count or rows // count > buf.shape[1]:
        count += 1
    return buf.at[pl.ds(0, count), pl.ds(0, rows // count)]


class Spread:
    def __init__(self, buf, starts, n, place, relayed, send, recv):
        self.buf, self.starts, self.n, self.place = buf, starts, n, place
        self.relayed, self.send, self.recv = relayed, send, recv

    def block(self, half, dp, dq):
        y, x = self.place
        dy, dx = (dq, dp) if half == 0 else (dp, dq)
        return lax.rem(y + dy + Y, Y), lax.rem(x + dx + X, X)

    def go(self, half, k, frm, to, part=None):
        y, x = self.block(half, *frm)
        start, count = self.starts[half], self.n
        if part is not None:
            count //= 2
            start += part * count
        ref = self.buf.at[y * X + x, pl.ds(start, count)]
        ty, tx = self.block(half, *to)
        pltpu.make_async_remote_copy(
            src_ref=ref,
            dst_ref=ref,
            send_sem=self.send,
            recv_sem=self.recv(k),
            device_id={"tp_0": ty, "tp_1": tx},
            device_id_type=MESH,
        ).start()

    def across(self, j):
        def straight():
            for half in range(2):
                self.go(half, 3, (j, 0), (0, 2))

        chosen(self.relayed, None, straight)
        for to in (1, -1):
            for half in range(2):
                self.go(half, 2 if j else 1, (j, 0), (0, to))

    def own(self):
        for to in (2, -1, 1):
            for half in range(2):
                self.go(half, 0, (0, 0), (to, 0))
        self.across(0)

    def first(self):
        self.got(0, 6)
        for j in (-1, 1, 2):
            self.across(j)

    def relay(self):
        for k, blocks, js in ((1, 4, (0,)), (2, 12, (-1, 1, 2))):
            self.got(k, blocks)

            def onward(js=js):
                for j in js:
                    for half in range(2):
                        self.go(half, 3, (j, -1), (0, 1), 0)
                        self.go(half, 3, (j, 1), (0, -1), 1)

            chosen(self.relayed, onward, None)

    def rest(self):
        self.got(3, 8)

    def got(self, k, blocks):
        landed(rows_in(self.buf, blocks * self.n), self.recv(k))


def whole_copy(region, sem):
    return pltpu.make_async_remote_copy(
        src_ref=region,
        dst_ref=region,
        send_sem=sem,
        recv_sem=sem,
        device_id={"tp_1": lax.rem(lax.axis_index("tp_1") + 1, X)},
        device_id_type=MESH,
    )


def landed(region, sem):
    whole_copy(region, sem).wait_recv()


def departed(region, sem):
    whole_copy(region, sem).wait_send()


def kernel(
    q_hbm, k_hbm, v_hbm, g_hbm, ld_hbm, wo_hbm, rows_hbm, gain_hbm, routes_hbm, rw_hbm,
    wg_hbm, wu_hbm, wd_hbm, cr_hbm, sr_hbm, cb_hbm, sb_hbm,
    mix_hbm, moe_hbm,
    q_ref, k_ref, v_ref, g_ref, ld_ref, rows_ref, gain_ref, routes_ref, rw_ref,
    cr_ref, sr_ref, cb_ref, sb_ref, mix_ref, moe_ref,
    wg, wu, wo, wa, wb, wt, oh, snd, rbuf, ha, hb, pa, pb, ra, rb, eo, ret,
    sts, str_, sto, sti, ins, rotq, cum, upd, ho, psum,
    lsem, send, recv, zsem,
):
    z, c = lax.axis_index("ep_0"), lax.axis_index("ep_1")
    y, x = lax.axis_index("tp_0"), lax.axis_index("tp_1")
    e = z * C + c
    t = y * X + x

    barrier = pltpu.get_barrier_semaphore()
    wd_rows = wd_hbm
    routed = (
        (routes_hbm, routes_ref), (rows_hbm, rows_ref), (gain_hbm, gain_ref), (rw_hbm, rw_ref),
    )
    mixed = (
        (k_hbm, k_ref), (q_hbm, q_ref), (v_hbm, v_ref), (ld_hbm, ld_ref), (cr_hbm, cr_ref),
        (sr_hbm, sr_ref), (cb_hbm.at[e], cb_ref), (sb_hbm.at[e], sb_ref), (g_hbm, g_ref),
    )
    held = (
        (wg_hbm, wg), (wu_hbm, wu), (wd_rows.at[y, :, 0], wa.at[y]),
        (wd_rows.at[:, x, 1], wb.at[x]), (wo_hbm, wo),
    )
    local = [
        pltpu.make_async_copy(src, dst, lsem.at[n])
        for n, (src, dst) in enumerate(routed + mixed + held)
    ]
    routed, mixed, local = (
        local[: len(routed)], local[len(routed) : -len(held)], local[-len(held) :],
    )
    for copy in routed:
        copy.start()

    def ring_dev(d):
        j = lax.rem(e + d, E)
        return j, {"ep_0": j // C, "ep_1": lax.rem(j, C)}

    def greet(d, _):
        pl.semaphore_signal(barrier, inc=1, device_id=ring_dev(d)[1], device_id_type=MESH)
        return _

    lax.fori_loop(1, E, greet, 0)
    for s in range(1, 4):
        pl.semaphore_signal(
            barrier, inc=1, device_id={"tp_0": lax.rem(y + s, Y)}, device_id_type=MESH
        )
        pl.semaphore_signal(
            barrier, inc=1, device_id={"tp_1": lax.rem(x + s, X)}, device_id_type=MESH
        )

    for copy in mixed + local:
        copy.start()

    for copy in routed:
        copy.wait()

    slot_id = lax.broadcasted_iota(jnp.int32, (SLOTS, ROWS), 0)
    expert_of = slot_id // CAP
    place_of = (slot_id - expert_of * CAP).astype(F32)
    named = [routes_ref[k : k + 1, :] == expert_of for k in range(2)]
    either = jnp.logical_or(named[0], named[1])
    before = (
        lax.broadcasted_iota(jnp.int32, (ROWS, ROWS), 0)
        < lax.broadcasted_iota(jnp.int32, (ROWS, ROWS), 1)
    )
    rank = mm(either.astype(F32).astype(BF16), before.astype(F32).astype(BF16))
    here = rank == place_of
    for k in range(2):
        oh[k] = jnp.logical_and(named[k], here).astype(F32).astype(BF16)

    lanes = pl.ds(pl.multiple_of(t * W, W), W)
    gain_at = lax.broadcasted_iota(jnp.int32, (T, W), 0) == t
    gain = jnp.sum(jnp.where(gain_at, gain_ref[...].astype(F32), 0.0), axis=0, keepdims=True)

    def squares(r, _):
        rows = pl.ds(pl.multiple_of(r * 64, 64), 64)
        full = rows_ref[rows, :].astype(F32)
        mean = jnp.sum(full * full, axis=-1, keepdims=True) * (1.0 / D)
        mine = rows_ref[rows, lanes].astype(F32)
        normed = mine * lax.rsqrt(mean + 1e-06) * gain
        rotq[rows, :] = normed.astype(BF16)
        return _

    lax.fori_loop(0, ROWS // 64, squares, 0)
    normed = rotq[...]
    picked = mm(oh[0] + oh[1], normed)
    snd[...] = picked.astype(BF16)
    mine_at = pl.ds(pl.multiple_of(e * CAP, CAP), CAP)
    own_rows = slice(OWN * CAP, (OWN + 1) * CAP)
    rbuf[t, own_rows, :] = snd[mine_at, :]

    pl.semaphore_wait(barrier, E - 1 + 6)

    def zigzag(i, low, high):
        even = 1 - lax.rem(i, 2)
        return even * (low + i // 2) + (1 - even) * (high - i // 2)

    def source_of(n, i):
        if n == 0:
            d = zigzag(i, -4, 3)
            return d, OWN + d
        if n == 1:
            return 15 - i, 15 - i
        if n == 2:
            return 16 + i, 16 + i
        d = zigzag(i, -8, 7)
        even = 1 - lax.rem(i, 2)
        return d, 20 + d + 16 * even

    def tile(k):
        return pl.ds(pl.multiple_of(k * CAP, CAP), CAP)

    def each(n, act):
        def step(i, carry):
            act(*source_of(n, i))
            return carry

        lax.fori_loop(0, 7 if n == 0 else 8, step, 0)

    for n in range(CHUNKS):

        def dispatch(d, slot, n=n):
            j, dev = ring_dev(E - d)
            pltpu.make_async_remote_copy(
                src_ref=snd.at[tile(j)],
                dst_ref=rbuf.at[t, tile(slot)],
                send_sem=zsem.at[0],
                recv_sem=zsem.at[8 + n],
                device_id=dev,
                device_id_type=MESH,
            ).start()

        each(n, dispatch)

    def weight_copy(src, dst, sem, axis, to):
        me = y if axis == "tp_0" else x
        pltpu.make_async_remote_copy(
            src_ref=src, dst_ref=dst, send_sem=send.at[0], recv_sem=recv.at[sem],
            device_id={axis: lax.rem(me + to + 4, 4)}, device_id_type=MESH,
        ).start()

    def down_rows(side, k, part=None):
        among = pl.ds(0, 4) if part is None else pl.ds(2 * part, 2)
        return wd_rows.at[k, among, 0] if side == 0 else wd_rows.at[among, k, 1]

    wsides = ((wa, "tp_0", y), (wb, "tp_1", x))
    for side, (into, axis, me) in enumerate(wsides):
        for part, to in ((0, 1), (1, -1)):
            weight_copy(down_rows(side, lax.rem(me + 2, 4), part), wt.at[side, part], 2, axis, to)
    for side, (into, axis, me) in enumerate(wsides):
        for to in (1, -1):
            weight_copy(down_rows(side, lax.rem(me + to + 4, 4)), into.at[me], side, axis, to)

    def relay_weights():
        landed(wt, recv.at[2])
        for side, (into, axis, me) in enumerate(wsides):
            for part, to in ((0, 1), (1, -1)):
                weight_copy(
                    wt.at[side, part], into.at[lax.rem(me - to + 4, 4), pl.ds(2 * part, 2)],
                    side, axis, to,
                )

    for copy in mixed:
        copy.wait()
    cb, sb = cb_ref[...], sb_ref[...]
    cos = cb * cr_ref[...] - sb * sr_ref[...]

    def signed(first, second):
        lane = lax.broadcasted_iota(jnp.int32, first.shape, 1)
        return jnp.where(lane < W // 2, -first, second)

    sin = sb * cr_ref[...] + cb * sr_ref[...]
    sin = signed(sin, sin)

    def turned(ref):
        full = ref[...].astype(F32)
        return full * cos + pltpu.roll(full, W // 2, 1) * sin

    rq = turned(q_ref).astype(BF16)
    rotq[...] = rq
    rk = (turned(k_ref) * (W**-0.5)).astype(BF16)
    row_i = lax.broadcasted_iota(jnp.int32, (BLOCK, BLOCK), 0)
    col_i = lax.broadcasted_iota(jnp.int32, (BLOCK, BLOCK), 1)
    causal = row_i >= col_i
    tri = causal.astype(F32).astype(BF16)
    ends = []
    for b in range(2):
        rows = slice(b * BLOCK, (b + 1) * BLOCK)
        decay = jnp.broadcast_to(ld_ref[b : b + 1, :], (BLOCK, BLOCK))
        column = jnp.zeros((BLOCK, BLOCK), F32)
        line = jnp.zeros((BLOCK, BLOCK), F32)
        for piece in parts_of(decay, 3):
            column = column + mm(tri, piece, 1, 1)
            line = line + mm(piece, tri, 1, 1)
        spread = column - line
        factor = jnp.where(causal, jnp.exp(jnp.where(causal, spread, 0.0)), 0.0)
        weights = (mm(rq[rows], rk[rows], 1, 1) * factor).astype(BF16)
        values = v_ref[rows, :]
        cum[rows, :] = column
        end = column[BLOCK - 1 : BLOCK, :]
        ends.append(end)
        scaled = rk[rows].astype(F32) * jnp.exp(end - column)
        high, low = parts_of(scaled, 2)
        upd[b] = mm(high, values, 0, 0) + mm(low, values, 0, 0)
        ins[rows, :] = mm(weights, values)
    whole = jnp.exp(ends[1]) * upd[0] + upd[1]
    total = ends[0] + ends[1]
    for s in range(Z):
        sts[s, 0:8, :] = whole[s * 8 : (s + 1) * 8, :]
        sts[s, 8:9, :] = total
    upd[1] = jnp.broadcast_to(jnp.exp(ends[0]), (BLOCK, W))

    owner = c == lax.rem(z, C)
    str_[e] = sts[z]

    def give(i, carry):
        s = lax.rem(z + i, Z)

        @pl.when(jnp.logical_or(i > 0, jnp.logical_not(owner)))
        def _():
            pltpu.make_async_remote_copy(
                src_ref=sts.at[s],
                dst_ref=str_.at[e],
                send_sem=zsem.at[4],
                recv_sem=zsem.at[5],
                device_id={"ep_0": s, "ep_1": lax.rem(s, C)},
                device_id_type=MESH,
            ).start()

        return carry

    lax.fori_loop(0, Z, give, 0)

    place = (y, x)
    moe = []
    for n in range(CHUNKS):
        moe.append(
            Spread(
                rbuf, (n * CHUNK, n * CHUNK + CHUNK // 2), CHUNK // 2, place, RELAY_ROWS[n],
                send.at[1], lambda k, n=n: recv.at[3 + 4 * n + k],
            )
        )
    mix = Spread(ho, (0, BLOCK), BLOCK, place, RELAY_HEADS, send.at[2], lambda k: recv.at[31 + k])

    def rows_of(n):
        return slice(n * CHUNK, (n + 1) * CHUNK), pl.ds(n * CHUNK, CHUNK)

    def arrive(n):
        count = 7 if n == 0 else 8
        landed(rbuf.at[t, pl.ds(0, count * CAP)], zsem.at[8 + n])
        moe[n].own()

    def hidden(n):
        moe[n].rest()
        rows, at = rows_of(n)
        left = jnp.concatenate([rbuf[k, rows, :] for k in range(T)], axis=1)
        units = (silu(mm(left, wg[...])) * mm(left, wu[...])).astype(BF16)
        ha[x, rows, :] = units[:, 0:W]
        hb[y, rows, :] = units[:, W : 2 * W]
        def straight():
            for side in range(2):
                hop(n, side, 0, 2)

        chosen(RELAY_HIDDEN[n], None, straight)
        for to in (1, -1):
            for side in range(2):
                hop(n, side, 0, to)

    hsides = ((ha, "tp_1", x), (hb, "tp_0", y))

    def hop(n, side, block, to, part=None):
        buf, axis, me = hsides[side]
        at = pl.ds(n * CHUNK, CHUNK)
        if part is not None:
            at = pl.ds(n * CHUNK + part * CHUNK // 2, CHUNK // 2)
        ref = buf.at[lax.rem(me + block + 4, 4), at]
        near = block == 0 and to != 2
        pltpu.make_async_remote_copy(
            src_ref=ref, dst_ref=ref, send_sem=send.at[3],
            recv_sem=recv.at[19 + 2 * n + (0 if near else 1)],
            device_id={axis: lax.rem(me + to + 4, 4)}, device_id_type=MESH,
        ).start()

    def hop_relay(n):
        landed(rows_in(ha, 4 * CHUNK), recv.at[19 + 2 * n])

        def onward():
            for side in range(2):
                hop(n, side, -1, 1, 0)
                hop(n, side, 1, -1, 1)

        chosen(RELAY_HIDDEN[n], onward, None)

    def down(n):
        landed(rows_in(ha, 2 * CHUNK), recv.at[20 + 2 * n])
        rows, at = rows_of(n)
        for side in range(2):
            buf, weight, out, into, axis, me = (
                (ha, wa, pa, ra, "tp_0", y), (hb, wb, pb, rb, "tp_1", x),
            )[side]
            left = jnp.concatenate([buf[k, rows, :] for k in range(4)], axis=1)
            right = jnp.concatenate(
                [weight[lax.rem(me + s, 4)].reshape(4 * W, W) for s in range(4)], axis=1
            )
            whole = mm(left, right)
            for s in (2, 1, 3):
                out[s - 1, rows, :] = whole[:, s * W : (s + 1) * W].astype(BF16)
                pltpu.make_async_remote_copy(
                    src_ref=out.at[s - 1, at], dst_ref=into.at[s - 1, at],
                    send_sem=send.at[4], recv_sem=recv.at[27 + n],
                    device_id={axis: lax.rem(me + s, 4)}, device_id_type=MESH,
                ).start()
            psum[side, rows, :] = whole[:, 0:W]

    def give_back(d, slot):
        pltpu.make_async_remote_copy(
            src_ref=eo.at[tile(slot)],
            dst_ref=ret.at[mine_at],
            send_sem=zsem.at[2],
            recv_sem=zsem.at[3],
            device_id=ring_dev(E + d)[1],
            device_id_type=MESH,
        ).start()

    def finish(n):
        landed(ra.at[pl.ds(0, 3), pl.ds(0, 2 * CHUNK)], recv.at[27 + n])
        rows, _ = rows_of(n)
        summed = psum[0, rows, :] + psum[1, rows, :]
        for into in (ra, rb):
            for s in range(3):
                summed = summed + into[s, rows, :].astype(F32)
        eo[rows, :] = summed.astype(BF16)
        if n == 0:
            ret[mine_at, :] = eo[own_rows, :]
        each(n, give_back)

    def scan_states():
        @pl.when(owner)
        def _():
            landed(str_.at[pl.ds(0, E - 1)], zsem.at[5])
            current = jnp.zeros((8, W), F32)
            for j in range(E):
                sto[j] = current
                if j + 1 < E:
                    current = jnp.exp(str_[j, 8:9, :]) * current + str_[j, 0:8, :]
            sti[z] = sto[e]

            def back(i, _):
                j, dev = ring_dev(i + 1)
                pltpu.make_async_remote_copy(
                    src_ref=sto.at[j],
                    dst_ref=sti.at[z],
                    send_sem=zsem.at[6],
                    recv_sem=zsem.at[7],
                    device_id=dev,
                    device_id_type=MESH,
                ).start()
                return _

            lax.fori_loop(0, E - 1, back, 0)

    def retain():
        @pl.when(owner)
        def _():
            landed(sti.at[pl.ds(0, Z - 1)], zsem.at[7])

        @pl.when(jnp.logical_not(owner))
        def _():
            landed(sti, zsem.at[7])

        entering = sti[...].reshape(W, W)
        for b in range(2):
            rows = slice(b * BLOCK, (b + 1) * BLOCK)
            high, low = parts_of(entering, 2)
            query = rotq[rows, :]
            carried = (mm(query, high) + mm(query, low)) * jnp.exp(cum[rows, :])
            retained = ins[rows, :] + carried
            mean = jnp.sum(retained * retained, axis=-1, keepdims=True) * (1.0 / W)
            gate = g_ref[rows, :].astype(F32)
            ho[t, rows, :] = (retained * lax.rsqrt(mean + 1e-05) * silu(gate)).astype(BF16)
            entering = upd[1] * entering + upd[0]

    def weights_here(n):
        for copy in local[:2]:
            copy.wait()

    def down_weights_here(n):
        for copy in local[2:4]:
            copy.wait()
        landed(wa.at[pl.ds(0, 3)], recv.at[0])
        landed(wb.at[pl.ds(0, 3)], recv.at[1])

    steps = {
        "O": arrive,
        "F": lambda n: moe[n].first(),
        "L": lambda n: moe[n].relay(),
        "U": weights_here,
        "H": hidden,
        "K": hop_relay,
        "V": down_weights_here,
        "D": down,
        "X": finish,
        "W": lambda n: relay_weights(),
        "S": lambda n: scan_states(),
        "R": lambda n: retain(),
        "M": lambda n: (mix.own, mix.first, mix.relay, mix.rest)[n](),
    }
    for name in ORDER:
        steps[name[0]](int(name[1]))
    local[4].wait()
    heads = jnp.concatenate([ho[k] for k in range(T)], axis=1)
    mix_ref[...] = mm(heads, wo[...]).astype(BF16)
    mix_out = pltpu.make_async_copy(mix_ref, mix_hbm, lsem.at[0])
    mix_out.start()

    landed(ret.at[pl.ds(0, (E - 1) * CAP)], zsem.at[3])
    moe_out = jnp.zeros((ROWS, W), F32)
    for k in range(2):
        share = jnp.transpose(jnp.broadcast_to(rw_ref[k : k + 1, :], (W, ROWS)))
        moe_out = moe_out + mm(oh[k], ret[...], 0, 0) * share
    moe_ref[...] = moe_out.astype(BF16)
    moe_copy = pltpu.make_async_copy(moe_ref, moe_hbm, lsem.at[1])
    moe_copy.start()

    for n, region in (
        (0, rbuf.at[pl.ds(0, 8)]), (1, rbuf.at[pl.ds(0, 15)]), (2, ho.at[pl.ds(0, 15)]),
        (3, rbuf.at[pl.ds(0, 6)]), (4, rbuf.at[pl.ds(0, 6)]),
    ):
        departed(region, send.at[n])
    departed(snd.at[pl.ds(0, (E - 1) * CAP)], zsem.at[0])
    departed(eo.at[pl.ds(0, (E - 1) * CAP)], zsem.at[2])

    @pl.when(owner)
    def _():
        departed(sts.at[pl.ds(0, Z - 1)], zsem.at[4])
        departed(sto.at[pl.ds(0, E - 1)], zsem.at[6])

    @pl.when(jnp.logical_not(owner))
    def _():
        departed(sts, zsem.at[4])

    mix_out.wait()
    moe_copy.wait()


def tables():
    half = W // 2
    inverse = 10000.0 ** (-np.arange(half, dtype=np.float64) / half)
    near = np.arange(ROWS, dtype=np.float64)[:, None] * inverse[None, :]
    base = (np.arange(E, dtype=np.float64) * ROWS)[:, None] * inverse[None, :]
    both_halves = lambda a: np.concatenate([a, a], axis=1).astype(np.float32)
    return (
        both_halves(np.cos(near)),
        both_halves(np.sin(near)),
        both_halves(np.cos(base))[:, None, :],
        both_halves(np.sin(base))[:, None, :],
    )


def on_device(
    queries, keys, values, gates, log_decay, out_weight,
    moe_rows, moe_gain, routes, route_weights, gate_proj, up_proj, down_proj,
):
    hbm = pl.BlockSpec(memory_space=pltpu.HBM)
    scratch = [
        pltpu.VMEM((ROWS, W), BF16),
        pltpu.VMEM((ROWS, W), BF16),
        pltpu.VMEM((ROWS, W), BF16),
        pltpu.VMEM((ROWS, W), BF16),
        pltpu.VMEM((2, BLOCK), F32),
        pltpu.VMEM((ROWS, D), BF16),
        pltpu.VMEM((T, W), BF16),
        pltpu.VMEM((2, ROWS), jnp.int32),
        pltpu.VMEM((2, ROWS), F32),
        pltpu.VMEM((ROWS, W), F32),
        pltpu.VMEM((ROWS, W), F32),
        pltpu.VMEM((1, W), F32),
        pltpu.VMEM((1, W), F32),
        pltpu.VMEM((ROWS, W), BF16),
        pltpu.VMEM((ROWS, W), BF16),
        pltpu.VMEM((D, 256), BF16),
        pltpu.VMEM((D, 256), BF16),
        pltpu.VMEM((D, W), BF16),
        pltpu.VMEM((Y, X, W, W), BF16),
        pltpu.VMEM((X, Y, W, W), BF16),
        pltpu.VMEM((2, 2, 2, W, W), BF16),
        pltpu.VMEM((2, SLOTS, ROWS), BF16),
        pltpu.VMEM((SLOTS, W), BF16),
        pltpu.VMEM((T, SLOTS, W), BF16),
        pltpu.VMEM((X, SLOTS, W), BF16),
        pltpu.VMEM((Y, SLOTS, W), BF16),
        pltpu.VMEM((3, SLOTS, W), BF16),
        pltpu.VMEM((3, SLOTS, W), BF16),
        pltpu.VMEM((3, SLOTS, W), BF16),
        pltpu.VMEM((3, SLOTS, W), BF16),
        pltpu.VMEM((SLOTS, W), BF16),
        pltpu.VMEM((SLOTS, W), BF16),
        pltpu.VMEM((Z, 9, W), F32),
        pltpu.VMEM((E, 9, W), F32),
        pltpu.VMEM((E, 8, W), F32),
        pltpu.VMEM((Z, 8, W), F32),
        pltpu.VMEM((ROWS, W), F32),
        pltpu.VMEM((ROWS, W), BF16),
        pltpu.VMEM((ROWS, W), F32),
        pltpu.VMEM((2, W, W), F32),
        pltpu.VMEM((T, ROWS, W), BF16),
        pltpu.VMEM((2, SLOTS, W), F32),
        pltpu.SemaphoreType.DMA((18,)),
        pltpu.SemaphoreType.DMA((5,)),
        pltpu.SemaphoreType.DMA((35,)),
        pltpu.SemaphoreType.DMA((12,)),
    ]
    out = jax.ShapeDtypeStruct((ROWS, W), BF16)
    return pl.pallas_call(
        kernel,
        out_shape=(out, out),
        in_specs=[hbm] * 17,
        out_specs=(hbm, hbm),
        scratch_shapes=scratch,
        compiler_params=pltpu.CompilerParams(
            collective_id=0, has_side_effects=True, vmem_limit_bytes=67043328
        ),
    )(
        queries, keys, values, gates, log_decay.reshape(2, BLOCK), out_weight,
        moe_rows, moe_gain.reshape(T, W), routes.T, route_weights.T,
        gate_proj.reshape(D, 256), up_proj.reshape(D, 256),
        down_proj.reshape(Y, X, 2, W, W), *tables(),
    )


def solution(mesh):
    torus = Mesh(mesh.devices.reshape(Z, C, Y, X), ("ep_0", "ep_1", "tp_0", "tp_1"))
    return jax.shard_map(
        on_device,
        mesh=torus,
        in_specs=(
            P(EP, TP), P(EP, TP), P(EP, TP), P(EP, TP), P(EP, TP), P(None, TP),
            P(EP, None), P(), P(EP, None), P(EP, None),
            P(EP, None, TP), P(EP, None, TP), P(EP, None, TP),
        ),
        out_specs=(P(EP, TP), P(EP, TP)),
        check_vma=False,
    )
```

time: 73.3 us -> 66 us (0.900)
  the two profiles are of different devices: /device:TPU:32 before, /device:TPU:1 now
where the time goes in v3:
time: 66 us; the launch traced here: 65.8 us
  Pallas kernels  63 us (95%)
  local copies, waits for them, and re-layouts  2.14 us (3%)
    pallas_call x1, Pallas kernels, on_device(): pl.pallas_call(kernel, out_shape=(out, out), in_specs=[hbm] * 17, out_spe...  63 us
    unnamed x4, local copies, waits for them, and re-layouts  2.14 us

profile of v3, /device:TPU:1, one launch (start us, length us, event | category | flops | bytes accessed | tf_op | source)
XLA Modules:
  0.0 65.8 jit_solution(13934448127555910382)
XLA Ops:
  0.6 63.0 %shard_map.176 = (bf16[256,128]{1,0:T(8,128)(2,1)}, bf16[256,128]{1,0:T(8,128)(2,1)}) custom-call(bf16[256,128]{1,0:T(8,128)(2,1)} %q_hbm.1, bf16[256,128]{1,0:T(8,128)(2,1)} %k_hbm.1, bf16[256,128]{1,0:T(8,128)(2,1)} %v_hbm.1, bf16[256,128]{1,0:T(8,128)(2,1)} %g_hbm.1, f32[2,128]{1,0:T(2,128)} %bitcast.13, bf16[2048,128]{1,0:T(8,128)(2,1)} %wo_hbm.1, ...), custom_call_target="tpu_custom_call" | custom-call | tf_op jit(solution)/shard_map/pallas_call | solution.py:677
  63.6 0.0 copy-start
  63.7 1.5 %copy.21 = bf16[256,128]{1,0:T(8,128)(2,1)} copy(bf16[256,128]{1,0:T(8,128)(2,1)} %get-tuple-element.4) | data formatting | bytes 131072
  65.2 0.0 copy-done
  65.2 0.6 copy.22
Async XLA Ops:
  63.6 1.5 %copy-start = (bf16[256,128]{1,0:T(8,128)(2,1)S(1)}, bf16[256,128]{1,0:T(8,128)(2,1)}, u32[]{:S(2)}) copy-start(bf16[256,128]{1,0:T(8,128)(2,1)} %get-tuple-element.5) | copy-start | bytes 196612

commit v4 on v3

--- a/solution.py
+++ b/solution.py
@@ -21,9 +21,9 @@
 BLOCK = 128
 CHUNKS = 4
 ORDER = (
-    "O0", "F0", "O1", "O2", "O3", "W0", "F1", "F2", "F3", "S0", "L0", "L1", "L2", "L3", "U0",
-    "H0", "H1", "H2", "H3", "R0", "M0", "V0", "K1", "D1", "K2", "D2", "K0", "D0", "K3", "D3",
-    "M1", "X1", "X2", "X0", "X3", "M2", "M3",
+    "O0", "O3", "G0", "F0", "O1", "O2", "W0", "F3", "F1", "F2", "L0", "S0", "L3", "L1", "L2",
+    "U0", "H0", "H1", "H2", "H3", "R0", "M0", "V0", "K1", "D1", "K2", "D2", "K0", "D0", "K3",
+    "D3", "X1", "M1", "X2", "X0", "X3", "M2", "M3",
 )
 RELAY_ROWS = (1, 1, 1, 1)
 RELAY_HIDDEN = (0, 0, 0, 0)
@@ -172,6 +172,11 @@
     t = y * X + x
 
     barrier = pltpu.get_barrier_semaphore()
+
+    def ring_dev(d):
+        j = lax.rem(e + d, E)
+        return j, {"ep_0": j // C, "ep_1": lax.rem(j, C)}
+
     wd_rows = wd_hbm
     routed = (
         (routes_hbm, routes_ref), (rows_hbm, rows_ref), (gain_hbm, gain_ref), (rw_hbm, rw_ref),
@@ -194,15 +199,11 @@
     for copy in routed:
         copy.start()
 
-    def ring_dev(d):
-        j = lax.rem(e + d, E)
-        return j, {"ep_0": j // C, "ep_1": lax.rem(j, C)}
-
-    def greet(d, _):
+    def greet(d):
         pl.semaphore_signal(barrier, inc=1, device_id=ring_dev(d)[1], device_id_type=MESH)
-        return _
-
-    lax.fori_loop(1, E, greet, 0)
+
+    for d in sorted(range(1, E), key=lambda d: -min(d, E - d)):
+        greet(d)
     for s in range(1, 4):
         pl.semaphore_signal(
             barrier, inc=1, device_id={"tp_0": lax.rem(y + s, Y)}, device_id_type=MESH
@@ -280,7 +281,7 @@
 
         lax.fori_loop(0, 7 if n == 0 else 8, step, 0)
 
-    for n in range(CHUNKS):
+    for n in (0, 3, 1, 2):
 
         def dispatch(d, slot, n=n):
             j, dev = ring_dev(E - d)
@@ -392,7 +393,8 @@
 
         return carry
 
-    lax.fori_loop(0, Z, give, 0)
+    def give_states():
+        lax.fori_loop(0, Z, give, 0)
 
     place = (y, x)
     moe = []
@@ -564,6 +566,7 @@
         "D": down,
         "X": finish,
         "W": lambda n: relay_weights(),
+        "G": lambda n: give_states(),
         "S": lambda n: scan_states(),
         "R": lambda n: retain(),
         "M": lambda n: (mix.own, mix.first, mix.relay, mix.rest)[n](),

time: 66 us -> 63.6 us (0.964)
  Pallas kernels: 63 us -> 60.6 us
    pallas_call x1, Pallas kernels: 63 us -> 60.6 us  [on_device(): pl.pallas_call(kernel, out_shape=(out, out), in_specs=[hbm] * 17, out_spe...]
where the time goes in v4:
time: 63.6 us; the launch traced here: 63.4 us
  Pallas kernels  60.6 us (95%)
  local copies, waits for them, and re-layouts  2.14 us (3%)
  between operations  0.65 us (1%)
    pallas_call x1, Pallas kernels, on_device(): pl.pallas_call(kernel, out_shape=(out, out), in_specs=[hbm] * 17, out_spe...  60.6 us
    unnamed x4, local copies, waits for them, and re-layouts  2.14 us

profile of v4, /device:TPU:1, one launch (start us, length us, event | category | flops | bytes accessed | tf_op | source)
XLA Modules:
  0.0 63.4 jit_solution(2308971774264177952)
XLA Ops:
  0.6 60.6 %shard_map.176 = (bf16[256,128]{1,0:T(8,128)(2,1)}, bf16[256,128]{1,0:T(8,128)(2,1)}) custom-call(bf16[256,128]{1,0:T(8,128)(2,1)} %q_hbm.1, bf16[256,128]{1,0:T(8,128)(2,1)} %k_hbm.1, bf16[256,128]{1,0:T(8,128)(2,1)} %v_hbm.1, bf16[256,128]{1,0:T(8,128)(2,1)} %g_hbm.1, f32[2,128]{1,0:T(2,128)} %bitcast.13, bf16[2048,128]{1,0:T(8,128)(2,1)} %wo_hbm.1, ...), custom_call_target="tpu_custom_call" | custom-call | tf_op jit(solution)/shard_map/pallas_call | solution.py:680
  61.3 0.0 copy-start
  61.3 1.5 %copy.21 = bf16[256,128]{1,0:T(8,128)(2,1)} copy(bf16[256,128]{1,0:T(8,128)(2,1)} %get-tuple-element.4) | data formatting | bytes 131072
  62.8 0.0 copy-done
  62.8 0.6 copy.22
Async XLA Ops:
  61.3 1.5 %copy-start = (bf16[256,128]{1,0:T(8,128)(2,1)S(1)}, bf16[256,128]{1,0:T(8,128)(2,1)}, u32[]{:S(2)}) copy-start(bf16[256,128]{1,0:T(8,128)(2,1)} %get-tuple-element.5) | copy-start | bytes 196612

commit v5 on v4

--- a/solution.py
+++ b/solution.py
@@ -21,7 +21,7 @@
 BLOCK = 128
 CHUNKS = 4
 ORDER = (
-    "O0", "O3", "G0", "F0", "O1", "O2", "W0", "F3", "F1", "F2", "L0", "S0", "L3", "L1", "L2",
+    "W0", "O0", "O3", "G0", "F0", "O1", "O2", "F3", "F1", "F2", "L0", "S0", "L3", "L1", "L2",
     "U0", "H0", "H1", "H2", "H3", "R0", "M0", "V0", "K1", "D1", "K2", "D2", "K0", "D0", "K3",
     "D3", "X1", "M1", "X2", "X0", "X3", "M2", "M3",
 )
@@ -159,10 +159,10 @@
 def kernel(
     q_hbm, k_hbm, v_hbm, g_hbm, ld_hbm, wo_hbm, rows_hbm, gain_hbm, routes_hbm, rw_hbm,
     wg_hbm, wu_hbm, wd_hbm, cr_hbm, sr_hbm, cb_hbm, sb_hbm,
-    mix_hbm, moe_hbm,
+    out_hbm,
     q_ref, k_ref, v_ref, g_ref, ld_ref, rows_ref, gain_ref, routes_ref, rw_ref,
     cr_ref, sr_ref, cb_ref, sb_ref, mix_ref, moe_ref,
-    wg, wu, wo, wa, wb, wt, oh, snd, rbuf, ha, hb, pa, pb, ra, rb, eo, ret,
+    wg, wu, wo, wa, wb, oh, snd, rbuf, ha, hb, pa, pb, ra, rb, eo, ret,
     sts, str_, sto, sti, ins, rotq, cum, upd, ho, psum,
     lsem, send, recv, zsem,
 ):
@@ -303,26 +303,16 @@
             device_id={axis: lax.rem(me + to + 4, 4)}, device_id_type=MESH,
         ).start()
 
-    def down_rows(side, k, part=None):
-        among = pl.ds(0, 4) if part is None else pl.ds(2 * part, 2)
-        return wd_rows.at[k, among, 0] if side == 0 else wd_rows.at[among, k, 1]
-
     wsides = ((wa, "tp_0", y), (wb, "tp_1", x))
-    for side, (into, axis, me) in enumerate(wsides):
-        for part, to in ((0, 1), (1, -1)):
-            weight_copy(down_rows(side, lax.rem(me + 2, 4), part), wt.at[side, part], 2, axis, to)
-    for side, (into, axis, me) in enumerate(wsides):
-        for to in (1, -1):
-            weight_copy(down_rows(side, lax.rem(me + to + 4, 4)), into.at[me], side, axis, to)
-
-    def relay_weights():
-        landed(wt, recv.at[2])
+
+    def send_weights(*shifts):
         for side, (into, axis, me) in enumerate(wsides):
-            for part, to in ((0, 1), (1, -1)):
-                weight_copy(
-                    wt.at[side, part], into.at[lax.rem(me - to + 4, 4), pl.ds(2 * part, 2)],
-                    side, axis, to,
-                )
+            for to in shifts:
+                k = lax.rem(me + to + 4, 4)
+                rows = wd_rows.at[k, :, 0] if side == 0 else wd_rows.at[:, k, 1]
+                weight_copy(rows, into.at[me], side, axis, to)
+
+    send_weights(1, -1)
 
     for copy in mixed:
         copy.wait()
@@ -565,7 +555,7 @@
         "V": down_weights_here,
         "D": down,
         "X": finish,
-        "W": lambda n: relay_weights(),
+        "W": lambda n: send_weights(2),
         "G": lambda n: give_states(),
         "S": lambda n: scan_states(),
         "R": lambda n: retain(),
@@ -576,7 +566,7 @@
     local[4].wait()
     heads = jnp.concatenate([ho[k] for k in range(T)], axis=1)
     mix_ref[...] = mm(heads, wo[...]).astype(BF16)
-    mix_out = pltpu.make_async_copy(mix_ref, mix_hbm, lsem.at[0])
+    mix_out = pltpu.make_async_copy(mix_ref, out_hbm.at[0], lsem.at[0])
     mix_out.start()
 
     landed(ret.at[pl.ds(0, (E - 1) * CAP)], zsem.at[3])
@@ -585,11 +575,11 @@
         share = jnp.transpose(jnp.broadcast_to(rw_ref[k : k + 1, :], (W, ROWS)))
         moe_out = moe_out + mm(oh[k], ret[...], 0, 0) * share
     moe_ref[...] = moe_out.astype(BF16)
-    moe_copy = pltpu.make_async_copy(moe_ref, moe_hbm, lsem.at[1])
+    moe_copy = pltpu.make_async_copy(moe_ref, out_hbm.at[1], lsem.at[1])
     moe_copy.start()
 
     for n, region in (
-        (0, rbuf.at[pl.ds(0, 8)]), (1, rbuf.at[pl.ds(0, 15)]), (2, ho.at[pl.ds(0, 15)]),
+        (0, rbuf.at[pl.ds(0, 6)]), (1, rbuf.at[pl.ds(0, 15)]), (2, ho.at[pl.ds(0, 15)]),
         (3, rbuf.at[pl.ds(0, 6)]), (4, rbuf.at[pl.ds(0, 6)]),
     ):
         departed(region, send.at[n])
@@ -649,7 +639,6 @@
         pltpu.VMEM((D, W), BF16),
         pltpu.VMEM((Y, X, W, W), BF16),
         pltpu.VMEM((X, Y, W, W), BF16),
-        pltpu.VMEM((2, 2, 2, W, W), BF16),
         pltpu.VMEM((2, SLOTS, ROWS), BF16),
         pltpu.VMEM((SLOTS, W), BF16),
         pltpu.VMEM((T, SLOTS, W), BF16),
@@ -676,12 +665,12 @@
         pltpu.SemaphoreType.DMA((35,)),
         pltpu.SemaphoreType.DMA((12,)),
     ]
-    out = jax.ShapeDtypeStruct((ROWS, W), BF16)
-    return pl.pallas_call(
+    out = jax.ShapeDtypeStruct((2, ROWS, W), BF16)
+    found = pl.pallas_call(
         kernel,
-        out_shape=(out, out),
+        out_shape=out,
         in_specs=[hbm] * 17,
-        out_specs=(hbm, hbm),
+        out_specs=hbm,
         scratch_shapes=scratch,
         compiler_params=pltpu.CompilerParams(
             collective_id=0, has_side_effects=True, vmem_limit_bytes=67043328
@@ -692,6 +681,7 @@
         gate_proj.reshape(D, 256), up_proj.reshape(D, 256),
         down_proj.reshape(Y, X, 2, W, W), *tables(),
     )
+    return found[0], found[1]
 
 
 def solution(mesh):

time: 63.6 us -> 62.8 us (0.987)
    unnamed x4 -> x0, local copies, waits for them, and re-layouts: 2.14 us -> none
    squeeze x0 -> x1, local copies, waits for them, and re-layouts: none -> 1.53 us  [on_device(): return (found[0], found[1])]
where the time goes in v5:
time: 62.8 us; the launch traced here: 62.6 us
  Pallas kernels  60.5 us (96%)
  local copies, waits for them, and re-layouts  1.53 us (2%)
  between operations  0.64 us (1%)
    pallas_call x1, Pallas kernels, on_device(): pl.pallas_call(kernel, out_shape=out, in_specs=[hbm] * 17, out_specs=hbm,...  60.5 us
    squeeze x1, local copies, waits for them, and re-layouts, on_device(): return (found[0], found[1])  1.53 us

profile of v5, /device:TPU:1, one launch (start us, length us, event | category | flops | bytes accessed | tf_op | source)
XLA Modules:
  0.0 62.6 jit_solution(7481541617262297730)
XLA Ops:
  0.6 60.5 %shard_map.176 = bf16[2,256,128]{2,1,0:T(8,128)(2,1)} custom-call(bf16[256,128]{1,0:T(8,128)(2,1)} %q_hbm.1, bf16[256,128]{1,0:T(8,128)(2,1)} %k_hbm.1, bf16[256,128]{1,0:T(8,128)(2,1)} %v_hbm.1, bf16[256,128]{1,0:T(8,128)(2,1)} %g_hbm.1, f32[2,128]{1,0:T(2,128)} %bitcast.17, bf16[2048,128]{1,0:T(8,128)(2,1)} %wo_hbm.1, bf16[256,2048]{1,0:T(8,128)(2,1)} %rows_hbm.1, ...), custom_call_target="tpu_custom_call" | custom-call | tf_op jit(solution)/shard_map/pallas_call | solution.py:669
  61.1 1.5 %slice_bitcast_fusion = (bf16[256,128]{1,0:T(8,128)(2,1)}, bf16[256,128]{1,0:T(8,128)(2,1)}) fusion(bf16[2,256,128]{2,1,0:T(8,128)(2,1)} %shard_map.176), kind=kLoop, calls=%fused_computation | loop fusion | bytes 262144 | tf_op jit(solution)/shard_map/squeeze | solution.py:684

commit v6 on v5

--- a/solution.py
+++ b/solution.py
@@ -163,7 +163,7 @@
     q_ref, k_ref, v_ref, g_ref, ld_ref, rows_ref, gain_ref, routes_ref, rw_ref,
     cr_ref, sr_ref, cb_ref, sb_ref, mix_ref, moe_ref,
     wg, wu, wo, wa, wb, oh, snd, rbuf, ha, hb, pa, pb, ra, rb, eo, ret,
-    sts, str_, sto, sti, ins, rotq, cum, upd, ho, psum,
+    sts, str_, sto, sti, ins, rotq, cum, upd, ho, psum, oht, share,
     lsem, send, recv, zsem,
 ):
     z, c = lax.axis_index("ep_0"), lax.axis_index("ep_1")
@@ -561,6 +561,10 @@
         "R": lambda n: retain(),
         "M": lambda n: (mix.own, mix.first, mix.relay, mix.rest)[n](),
     }
+    for k in range(2):
+        oht[k] = jnp.transpose(oh[k].astype(F32)).astype(BF16)
+        share[k] = jnp.transpose(jnp.broadcast_to(rw_ref[k : k + 1, :], (W, ROWS)))
+
     for name in ORDER:
         steps[name[0]](int(name[1]))
     local[4].wait()
@@ -572,8 +576,7 @@
     landed(ret.at[pl.ds(0, (E - 1) * CAP)], zsem.at[3])
     moe_out = jnp.zeros((ROWS, W), F32)
     for k in range(2):
-        share = jnp.transpose(jnp.broadcast_to(rw_ref[k : k + 1, :], (W, ROWS)))
-        moe_out = moe_out + mm(oh[k], ret[...], 0, 0) * share
+        moe_out = moe_out + mm(oht[k], ret[...]) * share[k]
     moe_ref[...] = moe_out.astype(BF16)
     moe_copy = pltpu.make_async_copy(moe_ref, out_hbm.at[1], lsem.at[1])
     moe_copy.start()
@@ -660,6 +663,8 @@
         pltpu.VMEM((2, W, W), F32),
         pltpu.VMEM((T, ROWS, W), BF16),
         pltpu.VMEM((2, SLOTS, W), F32),
+        pltpu.VMEM((2, ROWS, SLOTS), BF16),
+        pltpu.VMEM((2, ROWS, W), F32),
         pltpu.SemaphoreType.DMA((18,)),
         pltpu.SemaphoreType.DMA((5,)),
         pltpu.SemaphoreType.DMA((35,)),

time: 62.8 us -> 62.7 us (level)
  no operation moved by 1% of the time
where the time goes in v6:
time: 62.7 us; the launch traced here: 62.6 us
  Pallas kernels  60.4 us (96%)
  local copies, waits for them, and re-layouts  1.53 us (2%)
  between operations  0.64 us (1%)
    pallas_call x1, Pallas kernels, on_device(): pl.pallas_call(kernel, out_shape=out, in_specs=[hbm] * 17, out_specs=hbm,...  60.4 us
    squeeze x1, local copies, waits for them, and re-layouts, on_device(): return (found[0], found[1])  1.53 us

profile of v6, /device:TPU:1, one launch (start us, length us, event | category | flops | bytes accessed | tf_op | source)
XLA Modules:
  0.0 62.6 jit_solution(620283027721449187)
XLA Ops:
  0.6 60.4 %shard_map.176 = bf16[2,256,128]{2,1,0:T(8,128)(2,1)} custom-call(bf16[256,128]{1,0:T(8,128)(2,1)} %q_hbm.1, bf16[256,128]{1,0:T(8,128)(2,1)} %k_hbm.1, bf16[256,128]{1,0:T(8,128)(2,1)} %v_hbm.1, bf16[256,128]{1,0:T(8,128)(2,1)} %g_hbm.1, f32[2,128]{1,0:T(2,128)} %bitcast.17, bf16[2048,128]{1,0:T(8,128)(2,1)} %wo_hbm.1, bf16[256,2048]{1,0:T(8,128)(2,1)} %rows_hbm.1, ...), custom_call_target="tpu_custom_call" | custom-call | tf_op jit(solution)/shard_map/pallas_call | solution.py:674
  61.0 1.5 %slice_bitcast_fusion = (bf16[256,128]{1,0:T(8,128)(2,1)}, bf16[256,128]{1,0:T(8,128)(2,1)}) fusion(bf16[2,256,128]{2,1,0:T(8,128)(2,1)} %shard_map.176), kind=kLoop, calls=%fused_computation | loop fusion | bytes 262144 | tf_op jit(solution)/shard_map/squeeze | solution.py:689
